TPU v7x, 128 devices: a whole 4x4x4 slice. The times are simulated.
128 devices in a mesh: sp: 32 (over z, y, core), tp: 4 (over x).
Axes of the slice: x: 4, y: 4, z: 4, core: 2. Of those that a mesh axis runs over, the one named last changes fastest.
Arguments:
- tokens: bfloat16 [12288, 2048], P(('sp', 'tp')), may hold values from -8 to 8, as said below
- query_weight: bfloat16 [2048, 1024], P(None, 'tp'), as said below
- key_weight: bfloat16 [2048, 256], P(None, 'tp'), as said below
- value_weight: bfloat16 [2048, 256], P(None, 'tp'), may hold values from -0.125 to 0.125
- out_weight: bfloat16 [1024, 2048], P('tp'), may hold values from -0.75 to 0.75
- query_gain: bfloat16 [16, 64], P('tp'), may hold values from 0.5 to 6.5
- key_gain: bfloat16 [4, 64], P('tp'), may hold values from 0.5 to 6.5
Outputs:
- mixed: bfloat16 [12288, 2048], P(('sp', 'tp'))
- log_sums: float32 [16, 12288], P('tp', 'sp')
Inputs may be any that keep to these rules, and one draw needn't show every extreme that they name: Each block of 384 consecutive tokens has a mean vector of its own. `query_weight`: entries are those of a weight over 2048 inputs, of magnitude at most 6 / sqrt(2048). `key_weight`: entries are those of a weight over 2048 inputs, of magnitude at most 6 / sqrt(2048).
All inputs are finite; a program needn't handle non-finite values.
Results may differ from a plain program's by a relative error of at most 0.028.
Values may be sent and summed in bfloat16 or wider, within the bound.
No kernel may reach another device: no remote copies, remote signals or barrier semaphores. Data moves between devices by JAX's collectives and lax.ppermute only.
A program may use at most 64 MiB of HBM per device.

v0:
```python
import functools

import jax
import jax.numpy as jnp
import numpy as np
from jax import lax
from jax.experimental import pallas as pl
from jax.experimental.pallas import tpu as pltpu
from jax.sharding import PartitionSpec as P


ROPE_BASE = 10000.0
LOG2E = 1.4426950408889634
HEADROOM = 40.0
SUM_LOW = 2.0**-80
SUM_HIGH = 2.0**100
VMEM = pl.BlockSpec(memory_space=pltpu.VMEM)
QT = 768
KT = 768


def ring(n, k):
    return [(i, (i + k) % n) for i in range(n)]


def grid_move(step, first):
    pairs = []
    for s in range(32):
        z, y, c = s // 8, (s // 2) % 4, s % 2
        if (c == 0) == first:
            z = (z + step) % 4
        else:
            y = (y + step) % 4
        pairs.append((s, z * 8 + y * 2 + c))
    return pairs


def core_swap():
    return [(s, s ^ 1) for s in range(32)]


def dot(a, b):
    return lax.dot_general(a, b, (((1,), (0,)), ((), ())), preferred_element_type=jnp.float32)


def angle_rows(sp, tp, n):
    lane = lax.broadcasted_iota(jnp.int32, (64, 512), 1)
    row = lax.broadcasted_iota(jnp.int32, (64, 512), 0)
    again = lane >= 4 * n
    block = jnp.where(again, 3, lax.div(lane, n))
    inside = jnp.where(again, lane - 4 * n, lax.rem(lane, n))
    shift = jnp.where(block == 0, 0, jnp.where(block == 1, 3, jnp.where(block == 2, 1, 2)))
    place = sp * (4 * n) + ((tp + shift) & 3) * n + inside
    freq = jnp.asarray(np.tile(ROPE_BASE ** (-np.arange(16) / 16.0), 4)[:, None], jnp.float32)
    angle = jnp.where(row < 32, place >> 6, place & 63).astype(jnp.float32) * freq
    return jnp.where((row & 16) == 0, jnp.cos(angle), jnp.sin(angle))


def column(gain):
    eye = lax.broadcasted_iota(jnp.int32, (64, 64), 0) == lax.broadcasted_iota(jnp.int32, (64, 64), 1)
    wide = jnp.broadcast_to(gain.astype(jnp.float32), (64, 64))
    return jnp.sum(jnp.where(eye, wide, 0.0), axis=1, keepdims=True)


def norm_turn(x, gain, table):
    x = x * lax.rsqrt(jnp.mean(x * x, axis=0, keepdims=True) + 1e-06)
    x = x * gain
    rc, rs, cc, cs = table[0:16], table[16:32], table[32:48], table[48:64]
    a, b, c, d = x[0:16], x[16:32], x[32:48], x[48:64]
    return jnp.concatenate(
        [a * rc - b * rs, b * rc + a * rs, c * cc - d * cs, d * cc + c * cs], axis=0
    )


def keys_values(raw, gain, table):
    kv = raw.astype(jnp.float32).T
    keys = norm_turn(kv[0:64], gain, table)
    return jnp.concatenate([keys, kv[64:128]], axis=0).T.astype(jnp.bfloat16)


def own_kernel(place, t0, wq, wk, wv, wo, raw_ref, weight_ref, wo_ref):
    weight_ref[:, :256] = wq[...]
    weight_ref[:, 256:] = jnp.concatenate([wk[...], wv[...]], axis=0).astype(jnp.float32).T.astype(jnp.bfloat16)
    raw_ref[...] = dot(t0[...], weight_ref[...]).astype(jnp.bfloat16)
    half = wo_ref.shape[0]
    wo_ref[...] = wo[pl.ds(pl.multiple_of(place[0] * half, half), half), :]


def near_kernel(raw_own, t1, t2, weight, gk, tab, raw_ref, kv_ref, raw):
    n = t1.shape[0]
    raw[3 * n :, :] = jnp.zeros((n, 128), jnp.bfloat16)
    raw[:n, :] = raw_own[:, 256:]
    raw_ref[:n, :] = raw_own[:, :256]
    for i, t in ((1, t1), (2, t2)):
        made = dot(t[...], weight[...]).astype(jnp.bfloat16)
        raw[i * n : (i + 1) * n, :] = made[:, 256:]
        raw_ref[i * n : (i + 1) * n, :] = made[:, :256]
    kv_ref[...] = keys_values(raw[...], column(gk[...]), tab[:, : 4 * n])[: 3 * n]


def far_kernel(t3, t4, rawq, weight, gq, gk, tab, qt_ref, kv_ref, raw, raw_far):
    n = 2 * t3.shape[0]
    raw_far[n:, :] = jnp.zeros((128 - n, 128), jnp.bfloat16)
    made = dot(jnp.concatenate([t3[...], t4[...]], axis=0), weight[...]).astype(jnp.bfloat16)
    raw_far[:n, :] = made[:, 256:]
    kv_ref[...] = keys_values(raw_far[...], column(gk[...]), tab[:, 4 * n :])[:n]
    raw[: 3 * n, :] = rawq[...]
    raw[3 * n :, :] = made[:, :256]
    table = tab[:, : 4 * n]
    count = 4 * n
    for h in range(4):
        if h % 2 == 0:
            both = raw[:, h * 64 : h * 64 + 128].astype(jnp.float32).T
        x = both[(h % 2) * 64 : (h % 2) * 64 + 64]
        q = norm_turn(x, column(gq[h : h + 1, :]), table).astype(jnp.bfloat16)
        qt_ref[0:64, h * count : (h + 1) * count] = q
        qt_ref[64:128, h * count : (h + 1) * count] = jnp.zeros_like(q)


def join_kernel(*refs):
    *parts, out = refs
    at = 0
    for p in parts:
        out[at : at + p.shape[0], :] = p[...]
        at += p.shape[0]


def join(parts, size=None):
    size = size or parts[0].shape[0]
    rows = [min(size, p.shape[0]) for p in parts]
    specs = [pl.BlockSpec((r, 128), lambda i, b=p.shape[0] // r - 1: (b, 0)) for p, r in zip(parts, rows)]
    return pl.pallas_call(
        join_kernel,
        grid=(1,),
        out_shape=jax.ShapeDtypeStruct((sum(rows), 128), jnp.bfloat16),
        in_specs=specs,
        out_specs=pl.BlockSpec((sum(rows), 128), lambda i: (0, 0)),
        compiler_params=pltpu.CompilerParams(vmem_limit_bytes=4 * 2**20),
        cost_estimate=pl.CostEstimate(flops=1000, bytes_accessed=2**19, transcendentals=0),
    )(*parts)


def attend_kernel(*refs, n_kv, n_extra, first, last, scale, pieces):
    refs = list(refs)
    qt_ref = refs.pop(0)
    kv_refs = [refs.pop(0) for _ in range(n_kv)]
    extra = [refs.pop(0) for _ in range(n_extra)]
    if not first:
        acc_in, l_in, m_in = [refs.pop(0) for _ in range(3)]
    if last:
        att_refs = [refs.pop(0) for _ in range(4)]
        lse_ref = refs.pop(0)
        acc_ref, l_ref, m_ref = [refs.pop(0) for _ in range(3)]
    else:
        acc_ref, l_ref, m_ref = [refs.pop(0) for _ in range(3)]
    vt_ref, p_ref = refs
    c = scale * LOG2E
    nq = qt_ref.shape[1]

    def block(piece):
        parts = [kv_refs[j][r : r + size, :] for j, r, size in piece]
        return parts[0] if len(parts) == 1 else jnp.concatenate(parts, axis=0)

    for i, piece in enumerate(pieces):
        vt_ref[:, i * 384 : (i + 1) * 384] = block(piece).T[64:, :]

    for qi in range(nq // QT):
        cols = slice(qi * QT, (qi + 1) * QT)
        if first:
            top = None
            for piece in pieces:
                s = dot(block(piece)[:64], qt_ref[:, cols])
                s = jnp.max(s, axis=0, keepdims=True)
                top = s if top is None else jnp.maximum(top, s)
            m_ref[:, cols] = top * c + HEADROOM
            acc_ref[:, cols] = jnp.zeros((64, QT), jnp.float32)
            l_ref[:, cols] = jnp.zeros((8, QT), jnp.float32)
        else:
            m_ref[:, cols] = m_in[:, cols]
            acc_ref[:, cols] = acc_in[:, cols]
            l_ref[:, cols] = l_in[:, cols]

    def weigh(step, slot, cols):
        for h in range(2):
            s = dot(block(pieces[2 * step + h]), qt_ref[:, cols])
            p = jnp.exp2(s * c - m_ref[:, cols])
            l_ref[:, cols] += jnp.sum(p.reshape(48, 8, QT), axis=0)
            p_ref[slot, h * 384 : (h + 1) * 384, :] = p.astype(jnp.bfloat16)

    def gather_values(step, slot, cols):
        acc_ref[:, cols] += dot(vt_ref[:, step * 768 : (step + 1) * 768], p_ref[slot])

    steps = [
        (i, slice(qi * QT, (qi + 1) * QT)) for qi in range(nq // QT) for i in range(len(pieces) // 2)
    ]
    before = None
    for t, (i, cols) in enumerate(steps):
        weigh(i, t % 2, cols)
        if before is not None:
            gather_values(*before)
        before = (i, t % 2, cols)
    gather_values(*before)

    if last:
        total = jnp.sum(l_ref[...], axis=0, keepdims=True)
        good = jnp.logical_and(total > SUM_LOW, total < SUM_HIGH)
        n_bad = jnp.sum(jnp.where(good, 0.0, 1.0))

        @pl.when(n_bad > 0.0)
        def _():
            every = list(extra) + list(kv_refs)
            for qi in range(nq // 128):
                cols = slice(qi * 128, (qi + 1) * 128)
                m_ref[:, cols] = jnp.full((1, 128), -3e38, jnp.float32)
                acc_ref[:, cols] = jnp.zeros((64, 128), jnp.float32)
                l_ref[:, cols] = jnp.zeros((8, 128), jnp.float32)
            for kv in every:

                def top_of(i, _):
                    r = pl.multiple_of(i * 96, 96)
                    s = dot(kv[pl.ds(r, 96), :], qt_ref[...])
                    m_ref[...] = jnp.maximum(m_ref[...], jnp.max(s, axis=0, keepdims=True) * c)
                    return 0

                lax.fori_loop(0, kv.shape[0] // 96, top_of, 0)
            for kv in every:

                def again(i, _):
                    r = pl.multiple_of(i * 96, 96)
                    blk = kv[pl.ds(r, 96), :]
                    p = jnp.exp2(dot(blk, qt_ref[...]) * c - m_ref[...])
                    l_ref[...] += jnp.sum(p.reshape(12, 8, nq), axis=0)
                    acc_ref[...] += dot(blk.T[64:, :], p.astype(jnp.bfloat16))
                    return 0

                lax.fori_loop(0, kv.shape[0] // 96, again, 0)

        total = jnp.sum(l_ref[...], axis=0, keepdims=True)
        lse = (m_ref[...] + jnp.log2(total)) * (1.0 / LOG2E)
        out = acc_ref[...] / total
        count = nq // 4
        for h in range(0, 4, 2):
            two = jnp.concatenate(
                [out[:, h * count : (h + 1) * count], out[:, (h + 1) * count : (h + 2) * count]], axis=0
            )
            two = two.T.astype(jnp.bfloat16)
            for i, ref in enumerate(att_refs):
                ref[:, h * 64 : h * 64 + 128] = two[i * (count // 4) : (i + 1) * (count // 4)]
        for h in range(4):
            lse_ref[h : h + 1, :] = lse[:, h * count : (h + 1) * count]


def attend(qt, kvs, pieces, extra, state, last, scale):
    nq = qt.shape[1]
    keys = 384 * len(pieces)
    f32 = jnp.float32
    parts = (jax.ShapeDtypeStruct((64, nq), f32), jax.ShapeDtypeStruct((8, nq), f32), jax.ShapeDtypeStruct((1, nq), f32))
    scratch = [pltpu.VMEM((64, keys), jnp.bfloat16), pltpu.VMEM((2, KT, QT), jnp.bfloat16)]
    if last:
        outs = (jax.ShapeDtypeStruct((nq // 16, 256), jnp.bfloat16),) * 4 + (jax.ShapeDtypeStruct((4, nq // 4), f32),)
        scratch = [pltpu.VMEM(p.shape, f32) for p in parts] + scratch
    else:
        outs = parts
    args = [qt, *kvs, *extra, *(state or ())]
    return pl.pallas_call(
        functools.partial(
            attend_kernel, n_kv=len(kvs), n_extra=len(extra), first=state is None, last=last, scale=scale,
            pieces=pieces,
        ),
        out_shape=outs,
        in_specs=[VMEM] * len(args),
        out_specs=(VMEM,) * len(outs),
        scratch_shapes=scratch,
        compiler_params=pltpu.CompilerParams(vmem_limit_bytes=16 * 2**20),
        cost_estimate=pl.CostEstimate(
            flops=4 * nq * keys * 64, bytes_accessed=keys * 256 + nq * 512, transcendentals=nq * keys
        ),
    )(*args)


def mix_kernel(place, lse, a0, a1, a2, a3, w0, w1, w2, w3, x1, x2, x3, out_ref, lse_ref):
    half = w1.shape[0]
    here = pl.ds(pl.multiple_of(place[0] * half, half), half)
    there = pl.ds(pl.multiple_of((1 - place[0]) * half, half), half)
    total = dot(a0[...], w0[...])
    for a, w, x in ((a1, w1, x1), (a2, w2, x2), (a3, w3, x3)):
        total += dot(a[:, here], w[...]) + dot(a[:, there], x[...])
    out_ref[...] = total.astype(jnp.bfloat16)
    n = lse.shape[1] // 4
    cyc = [lse[:, i * n : (i + 1) * n] for i in (0, 2, 3, 1)]
    for t in range(4):

        @pl.when(place[1] == t)
        def _():
            lse_ref[...] = jnp.concatenate([cyc[(a - t) % 4] for a in range(4)], axis=1)


def body(tokens, query_weight, key_weight, value_weight, out_weight, query_gain, key_gain):
    scale = query_gain.shape[1] ** (-0.5)
    n = tokens.shape[0]
    sp, tp = lax.axis_index("sp"), lax.axis_index("tp")
    place = jnp.stack([sp & 1, tp])
    bf16 = jnp.bfloat16
    small = pltpu.CompilerParams(vmem_limit_bytes=12 * 2**20)

    def cost(tokens_done):
        return pl.CostEstimate(flops=2 * tokens_done * 2048 * 384, bytes_accessed=2**22, transcendentals=0)

    from_left = lax.ppermute(tokens, "tp", ring(4, 1))
    from_right = lax.ppermute(tokens, "tp", ring(4, 3))
    far_a = lax.ppermute(from_left[: n // 2], "tp", ring(4, 1))
    far_b = lax.ppermute(from_right[n // 2 :], "tp", ring(4, 3))
    table = angle_rows(sp, tp, n)
    half = out_weight.shape[0] // 2
    raw_own, weight, mine = pl.pallas_call(
        own_kernel,
        out_shape=(
            jax.ShapeDtypeStruct((n, 384), bf16),
            jax.ShapeDtypeStruct((2048, 384), bf16),
            jax.ShapeDtypeStruct((half, out_weight.shape[1]), bf16),
        ),
        in_specs=[pl.BlockSpec(memory_space=pltpu.SMEM)] + [VMEM] * 5,
        out_specs=(VMEM,) * 3,
        compiler_params=small,
        cost_estimate=cost(n),
    )(place, tokens, query_weight, key_weight.T, value_weight.T, out_weight)
    rawq, kv_near = pl.pallas_call(
        near_kernel,
        out_shape=(jax.ShapeDtypeStruct((3 * n, 256), bf16), jax.ShapeDtypeStruct((3 * n, 128), bf16)),
        in_specs=[VMEM] * 6,
        out_specs=(VMEM, VMEM),
        scratch_shapes=[pltpu.VMEM((4 * n, 128), bf16)],
        compiler_params=small,
        cost_estimate=cost(3 * n),
    )(raw_own, from_left, from_right, weight, key_gain, table)
    line = [kv_near]
    for k in (1, 3, 2):
        line.append(lax.ppermute(kv_near, "sp", grid_move(k, True)))
    qt, kv_far = pl.pallas_call(
        far_kernel,
        out_shape=(jax.ShapeDtypeStruct((128, 16 * n), bf16), jax.ShapeDtypeStruct((n, 128), bf16)),
        in_specs=[VMEM] * 7,
        out_specs=(VMEM, VMEM),
        scratch_shapes=[pltpu.VMEM((4 * n, 256), bf16), pltpu.VMEM((128, 128), bf16)],
        compiler_params=small,
        cost_estimate=cost(n),
    )(far_a, far_b, rawq, weight, query_gain, key_gain, table)

    load = join([*line, kv_far])
    twin = [lax.ppermute(load, "sp", core_swap())]
    got = [load]
    for k in (1, 3, 2):
        got.append(lax.ppermute(load, "sp", grid_move(k, False)))
    twin += [lax.ppermute(p, "sp", core_swap()) for p in got[1:]]
    line_far = join(got, n)
    rest = []
    for k in (1, 3, 2):
        rest.append(lax.ppermute(line_far, "sp", grid_move(k, True)))
    twin_rest = [lax.ppermute(p, "sp", core_swap()) for p in rest]

    mine, _ = lax.optimization_barrier((mine, kv_near))
    rows_in = []
    for k in (1, 3, 2):
        rows_in.append(lax.ppermute(mine, "tp", ring(4, k)))

    def thirds(j):
        return [((j, 384 * i, 384),) for i in range(3)]

    tails = tuple((j, 1152, 96) for j in range(4))
    state = attend(qt, [got[0], twin[0]], thirds(0) + thirds(1), [], None, False, scale)
    state = attend(qt, got, thirds(1) + thirds(2) + thirds(3) + [tails], [], state, False, scale)
    state = attend(qt, twin, thirds(1) + thirds(2) + thirds(3) + [tails], [], state, False, scale)
    *rows_in, _ = lax.optimization_barrier((*rows_in, state[2]))
    rows_other = [lax.ppermute(w, "sp", core_swap()) for w in rows_in]
    ends = [((j, 0, 384),) for j in range(6)]
    *att, lse = attend(qt, rest + twin_rest, ends, got + twin, state, True, scale)
    back = [lax.ppermute(att[i], "tp", ring(4, k)) for i, k in ((2, 1), (1, 3), (3, 2))]
    return pl.pallas_call(
        mix_kernel,
        out_shape=(jax.ShapeDtypeStruct((n, out_weight.shape[1]), bf16), jax.ShapeDtypeStruct((4, 4 * n), jnp.float32)),
        in_specs=[pl.BlockSpec(memory_space=pltpu.SMEM)] + [VMEM] * 12,
        out_specs=(VMEM, VMEM),
        compiler_params=small,
        cost_estimate=pl.CostEstimate(flops=2 * n * 1024 * 2048, bytes_accessed=2**22, transcendentals=0),
    )(place, lse, att[0], *back, out_weight, *rows_in, *rows_other)


def solution(mesh):
    return jax.shard_map(
        body,
        mesh=mesh,
        in_specs=(
            P(("sp", "tp"), None),
            P(None, "tp"),
            P(None, "tp"),
            P(None, "tp"),
            P("tp", None),
            P("tp", None),
            P("tp", None),
        ),
        out_specs=(P(("sp", "tp"), None), P("tp", "sp")),
        check_vma=False,
    )
```

profile of v0, /device:TPU:0, one launch (start us, length us, event | category | flops | bytes accessed | tf_op | source)
XLA Modules:
  0.0 185.8 jit_solution(14187547601848573443)
XLA Ops:
  0.6 1.7 collective-permute-start
  2.3 1.6 collective-permute-start.2
  4.0 1.2 sine_select_fusion.tab
  5.2 7.7 %collective-permute-done.t1 = bf16[96,2048]{1,0:T(8,128)(2,1)S(1)} collective-permute-done((bf16[96,2048]{1,0:T(8,128)(2,1)}, bf16[96,2048]{1,0:T(8,128)(2,1)S(1)}, u32[]{:S(2)}, u32[]{:S(2)}) %collective-permute-start) | collective-permute-done | bytes 393248 | tf_op jit(solution)/shard_map/ppermute | solution.py:309
  12.9 0.5 collective-permute-start.1
  13.5 0.0 collective-permute-done.2.t2
  13.5 0.0 copy-start.6
  13.5 2.8 %collective-permute-start.3 = (bf16[48,2048]{1,0:T(8,128)(2,1)S(1)}, bf16[48,2048]{1,0:T(8,128)(2,1)S(1)}, u32[]{:S(2)}, u32[]{:S(2)}) collective-permute-start(bf16[48,2048]{1,0:T(8,128)(2,1)S(1)} %slice.9), channel_id=1, source_target_pairs={{0,3},{1,0},{2,1},{3,2},{4,7},{5,4},{6,5},{7,6},{8,11},{9,8},{10,9... | collective-permute-start | bytes 589832 | tf_op jit(solution)/shard_map/ppermute | solution.py:312
  16.3 0.1 pad_add_fusion.place
  16.4 1.2 copy-done
  17.6 1.2 copy-done.2
  18.8 1.0 copy-done.3
  19.8 0.9 copy-done.4
  20.8 0.9 copy-done.5
  21.7 1.1 shard_map.95
  22.8 0.0 copy-start.7
  22.8 0.9 shard_map.96
  23.7 4.1 %collective-permute-start.6 = (bf16[288,128]{1,0:T(8,128)(2,1)S(1)}, bf16[288,128]{1,0:T(8,128)(2,1)S(1)}, u32[]{:S(2)}, u32[]{:S(2)}) collective-permute-start(bf16[288,128]{1,0:T(8,128)(2,1)S(1)} %get-tuple-element.31.refs_0_), channel_id=1, source_target_pairs={{0,64},{4,20},{8,72},{12,28},{16,80},{20,4},{24,88},{28,12},{32,96... | collective-permute-start | bytes 221192 | tf_op jit(solution)/shard_map/ppermute | solution.py:338
  27.8 0.7 collective-permute-start.5
  28.5 1.3 collective-permute-start.4
  29.9 0.0 collective-permute-done.1.t3
  29.9 0.0 collective-permute-done.3.t4
  29.9 0.7 shard_map.97
  30.5 0.0 collective-permute-done.6.refs_3_
  30.5 1.6 collective-permute-done.5.refs_2_
  32.2 1.9 %collective-permute-done.4.refs_1_ = bf16[288,128]{1,0:T(8,128)(2,1)S(1)} collective-permute-done((bf16[288,128]{1,0:T(8,128)(2,1)S(1)}, bf16[288,128]{1,0:T(8,128)(2,1)S(1)}, u32[]{:S(2)}, u32[]{:S(2)}) %collective-permute-start.4) | collective-permute-done | bytes 73760 | tf_op jit(solution)/shard_map/ppermute | solution.py:338
  34.1 6.4 %collective-permute-start.9 = (bf16[1248,128]{1,0:T(8,128)(2,1)S(1)}, bf16[1248,128]{1,0:T(8,128)(2,1)S(1)}, u32[]{:S(2)}, u32[]{:S(2)}) collective-permute-start(bf16[1248,128]{1,0:T(8,128)(2,1)S(1)} %shard_map.98.refs_0_.refs_1_.refs_7_), channel_id=1, source_target_pairs={{0,16},{4,68},{8,24},{12,76},{16,0},{20,84},{24,8},{28,92},{32,48}... | collective-permute-start | bytes 958472 | tf_op jit(solution)/shard_map/ppermute | solution.py:353
  40.5 0.0 collective-permute-start.16
  40.5 1.4 collective-permute-start.8
  41.9 0.7 collective-permute-start.7
  42.6 2.9 %collective-permute-done.9.refs_3_.refs_4_.refs_10_ = bf16[1248,128]{1,0:T(8,128)(2,1)S(1)} collective-permute-done((bf16[1248,128]{1,0:T(8,128)(2,1)S(1)}, bf16[1248,128]{1,0:T(8,128)(2,1)S(1)}, u32[]{:S(2)}, u32[]{:S(2)}) %collective-permute-start.9) | collective-permute-done | bytes 319520 | tf_op jit(solution)/shard_map/ppermute | solution.py:353
  45.5 0.0 collective-permute-start.19
  45.5 0.6 collective-permute-start.25
  46.1 0.0 collective-permute-done.16.refs_2_.refs_1_.refs_11_
  46.1 1.2 collective-permute-start.24
  47.3 2.4 %collective-permute-done.8.refs_2_.refs_3_.refs_9_ = bf16[1248,128]{1,0:T(8,128)(2,1)S(1)} collective-permute-done((bf16[1248,128]{1,0:T(8,128)(2,1)S(1)}, bf16[1248,128]{1,0:T(8,128)(2,1)S(1)}, u32[]{:S(2)}, u32[]{:S(2)}) %collective-permute-start.8) | collective-permute-done | bytes 319520 | tf_op jit(solution)/shard_map/ppermute | solution.py:353
  49.6 0.4 collective-permute-done.7.refs_1_.refs_2_.refs_8_
  50.1 0.0 collective-permute-done.19.refs_4_.refs_14_
  50.1 0.5 collective-permute-start.17
  50.6 3.5 %shard_map.100 = (f32[64,1536]{1,0:T(8,128)S(1)}, f32[8,1536]{1,0:T(8,128)S(1)}, f32[1,1536]{1,0:T(1,128)S(1)}) custom-call(bf16[128,1536]{1,0:T(8,128)(2,1)S(1)} %get-tuple-element.30.refs_0_, bf16[1248,128]{1,0:T(8,128)(2,1)S(1)} %shard_map.98.refs_0_.refs_1_.refs_7_, bf16[1248,128]{1,0:T(8,128)(2,1)S(1)} %collective-permute-done.16.refs_2_.refs_1_.refs_11_), custom_call_target="tpu_custom_call" | custom-call | flops 905969664 | bytes 1376256 | tf_op jit(solution)/shard_map/pallas_call | solution.py:265
  54.1 5.3 %shard_map.101 = (f32[64,1536]{1,0:T(8,128)S(1)}, f32[8,1536]{1,0:T(8,128)S(1)}, f32[1,1536]{1,0:T(1,128)S(1)}) custom-call(bf16[128,1536]{1,0:T(8,128)(2,1)S(1)} %get-tuple-element.30.refs_0_, bf16[1248,128]{1,0:T(8,128)(2,1)S(1)} %shard_map.98.refs_0_.refs_1_.refs_7_, bf16[1248,128]{1,0:T(8,128)(2,1)S(1)} %collective-permute-done.7.refs_1_.refs_2_.refs_8_, ...), custom_call_target="tpu_custom_call" | custom-call | flops 1509949440 | bytes 1769472 | tf_op jit(solution)/shard_map/pallas_call | solution.py:265
  59.4 0.0 collective-permute-done.18.refs_3_.refs_13_
  59.5 0.0 collective-permute-done.17.refs_2_.refs_12_
  59.5 5.6 %shard_map.102 = (f32[64,1536]{1,0:T(8,128)S(1)}, f32[8,1536]{1,0:T(8,128)S(1)}, f32[1,1536]{1,0:T(1,128)S(1)}) custom-call(bf16[128,1536]{1,0:T(8,128)(2,1)S(1)} %get-tuple-element.30.refs_0_, bf16[1248,128]{1,0:T(8,128)(2,1)S(1)} %collective-permute-done.16.refs_2_.refs_1_.refs_11_, bf16[1248,128]{1,0:T(8,128)(2,1)S(1)} %collective-permute-done.17.refs_2_.refs_12_, ...), custom_call_target="tpu_custom_call" | custom-call | flops 1509949440 | bytes 1769472 | tf_op jit(solution)/shard_map/pallas_call | solution.py:265
  65.0 5.2 %collective-permute-done.24.w2 = bf16[128,2048]{1,0:T(8,128)(2,1)S(1)} collective-permute-done((bf16[128,2048]{1,0:T(8,128)(2,1)S(1)}, bf16[128,2048]{1,0:T(8,128)(2,1)S(1)}, u32[]{:S(2)}, u32[]{:S(2)}) %collective-permute-start.24) | collective-permute-done | bytes 524320 | tf_op jit(solution)/shard_map/ppermute | solution.py:364
  70.3 2.3 %collective-permute-done.23.w1 = bf16[128,2048]{1,0:T(8,128)(2,1)S(1)} collective-permute-done((bf16[128,2048]{1,0:T(8,128)(2,1)S(1)}, bf16[128,2048]{1,0:T(8,128)(2,1)S(1)}, u32[]{:S(2)}, u32[]{:S(2)}) %collective-permute-start.23) | collective-permute-done | bytes 524320 | tf_op jit(solution)/shard_map/ppermute | solution.py:364
  72.6 0.0 collective-permute-start.26
  72.6 0.5 collective-permute-start.27
  73.1 0.0 collective-permute-start.28
  73.1 0.1 collective-permute-start.12
  73.2 0.1 collective-permute-start.11
  73.3 6.0 %collective-permute-done.12.refs_3_ = bf16[384,128]{1,0:T(8,128)(2,1)S(1)} collective-permute-done((bf16[384,128]{1,0:T(8,128)(2,1)S(1)}, bf16[384,128]{1,0:T(8,128)(2,1)S(1)}, u32[]{:S(2)}, u32[]{:S(2)}) %collective-permute-start.12) | collective-permute-done | bytes 98336 | tf_op jit(solution)/shard_map/ppermute | solution.py:358
  79.3 0.0 collective-permute-start.10
  79.3 1.7 collective-permute-start.15
  81.0 4.2 %collective-permute-done.10.refs_1_ = bf16[384,128]{1,0:T(8,128)(2,1)S(1)} collective-permute-done((bf16[384,128]{1,0:T(8,128)(2,1)S(1)}, bf16[384,128]{1,0:T(8,128)(2,1)S(1)}, u32[]{:S(2)}, u32[]{:S(2)}) %collective-permute-start.10) | collective-permute-done | bytes 98336 | tf_op jit(solution)/shard_map/ppermute | solution.py:358
  85.1 0.5 collective-permute-start.13
  85.6 0.8 collective-permute-done.14.refs_5_
  86.4 0.2 collective-permute-done.13.refs_4_
  86.6 85.9 %shard_map.103 = (bf16[96,256]{1,0:T(8,128)(2,1)S(1)}, bf16[96,256]{1,0:T(8,128)(2,1)S(1)}, bf16[96,256]{1,0:T(8,128)(2,1)S(1)}, bf16[96,256]{1,0:T(8,128)(2,1)S(1)}, f32[4,384]{1,0:T(4,128)S(1)}) custom-call(bf16[128,1536]{1,0:T(8,128)(2,1)S(1)} %get-tuple-element.30.refs_0_, bf16[384,128]{1,0:T(8,128)(2,1)S(1)} %collective-permute-done.10.refs_1_, ...), custom_call_target="tpu_custom_call" | custom-call | flops 905969664 | bytes 1376256 | tf_op jit(solution)/shard_map/pallas_call | solution.py:265
  172.5 0.1 collective-permute-start.20
  172.6 3.2 %collective-permute-start.21 = (bf16[96,256]{1,0:T(8,128)(2,1)S(1)}, bf16[96,256]{1,0:T(8,128)(2,1)S(1)}, u32[]{:S(2)}, u32[]{:S(2)}) collective-permute-start(bf16[96,256]{1,0:T(8,128)(2,1)S(1)} %get-tuple-element.45), channel_id=1, source_target_pairs={{0,3},{1,0},{2,1},{3,2},{4,7},{5,4},{6,5},{7,6},{8,11},{9,8},{10,9... | collective-permute-start | bytes 147464 | tf_op jit(solution)/shard_map/ppermute | solution.py:377
  175.8 2.1 %collective-permute-done.20.a1 = bf16[96,256]{1,0:T(8,128)(2,1)S(1)} collective-permute-done((bf16[96,256]{1,0:T(8,128)(2,1)S(1)}, bf16[96,256]{1,0:T(8,128)(2,1)S(1)}, u32[]{:S(2)}, u32[]{:S(2)}) %collective-permute-start.20) | collective-permute-done | bytes 49184 | tf_op jit(solution)/shard_map/ppermute | solution.py:377
  177.9 5.6 %collective-permute-done.22.a3 = bf16[96,256]{1,0:T(8,128)(2,1)S(1)} collective-permute-done((bf16[96,256]{1,0:T(8,128)(2,1)S(1)}, bf16[96,256]{1,0:T(8,128)(2,1)S(1)}, u32[]{:S(2)}, u32[]{:S(2)}) %collective-permute-start.22) | collective-permute-done | bytes 49184 | tf_op jit(solution)/shard_map/ppermute | solution.py:377
  183.5 2.3 %shard_map.104 = (bf16[96,2048]{1,0:T(8,128)(2,1)}, f32[4,384]{1,0:T(4,128)}) custom-call(s32[2]{0:T(128)S(1)} %pad_add_fusion.place, f32[4,384]{1,0:T(4,128)S(1)} %get-tuple-element.42.lse, bf16[96,256]{1,0:T(8,128)(2,1)S(1)} %get-tuple-element.43.a0, bf16[96,256]{1,0:T(8,128)(2,1)S(1)} %collective-permute-done.20.a1, ...), custom_call_target="tpu_custom_call" | custom-call | flops 402653184 | bytes 4194304 | tf_op jit(solution)/shard_map/pallas_call | solution.py:378
  (28 shorter events, 0.1 us)
Async XLA Ops:
  0.6 12.3 %collective-permute-start = (bf16[96,2048]{1,0:T(8,128)(2,1)}, bf16[96,2048]{1,0:T(8,128)(2,1)S(1)}, u32[]{:S(2)}, u32[]{:S(2)}) collective-permute-start(bf16[96,2048]{1,0:T(8,128)(2,1)} %t0.1), channel_id=1, source_target_pairs={{0,1},{1,2},{2,3},{3,0},{4,5},{5,6},{6,7},{7,4},{8,9},{9,10},{10,1... | collective-permute-start | bytes 1179656 | tf_op jit(solution)/shard_map/ppermute | solution.py:309
  2.3 11.2 %collective-permute-start.2 = (bf16[96,2048]{1,0:T(8,128)(2,1)}, bf16[96,2048]{1,0:T(8,128)(2,1)S(1)}, u32[]{:S(2)}, u32[]{:S(2)}) collective-permute-start(bf16[96,2048]{1,0:T(8,128)(2,1)} %t0.1), channel_id=1, source_target_pairs={{0,3},{1,0},{2,1},{3,2},{4,7},{5,4},{6,5},{7,6},{8,11},{9,8},{10,9... | collective-permute-start | bytes 1179656 | tf_op jit(solution)/shard_map/ppermute | solution.py:310
  12.9 16.9 %collective-permute-start.1 = (bf16[48,2048]{1,0:T(8,128)(2,1)S(1)}, bf16[48,2048]{1,0:T(8,128)(2,1)S(1)}, u32[]{:S(2)}, u32[]{:S(2)}) collective-permute-start(bf16[48,2048]{1,0:T(8,128)(2,1)S(1)} %slice.8), channel_id=1, source_target_pairs={{0,1},{1,2},{2,3},{3,0},{4,5},{5,6},{6,7},{7,4},{8,9},{9,10},{10,1... | collective-permute-start | bytes 589832 | tf_op jit(solution)/shard_map/ppermute | solution.py:311
  13.5 9.3 %copy-start.6 = (bf16[1,64]{1,0:T(2,128)(2,1)S(1)}, bf16[1,64]{1,0:T(2,128)(2,1)}, u32[]{:S(2)}) copy-start(bf16[1,64]{1,0:T(2,128)(2,1)} %gk.3) | copy-start | bytes 388
  13.5 16.4 %collective-permute-start.3 = (bf16[48,2048]{1,0:T(8,128)(2,1)S(1)}, bf16[48,2048]{1,0:T(8,128)(2,1)S(1)}, u32[]{:S(2)}, u32[]{:S(2)}) collective-permute-start(bf16[48,2048]{1,0:T(8,128)(2,1)S(1)} %slice.9), channel_id=1, source_target_pairs={{0,3},{1,0},{2,1},{3,2},{4,7},{5,4},{6,5},{7,6},{8,11},{9,8},{10,9... | collective-permute-start | bytes 589832 | tf_op jit(solution)/shard_map/ppermute | solution.py:312
  16.4 1.2 copy-start
  17.6 1.2 copy-start.2
  18.8 1.0 copy-start.3
  19.8 0.9 copy-start.4
  20.8 0.9 copy-start.5
  22.8 7.1 %copy-start.7 = (bf16[4,64]{1,0:T(4,128)(2,1)S(1)}, bf16[4,64]{1,0:T(4,128)(2,1)}, u32[]{:S(2)}) copy-start(bf16[4,64]{1,0:T(4,128)(2,1)} %gq.1) | copy-start | bytes 1540
  23.7 6.8 %collective-permute-start.6 = (bf16[288,128]{1,0:T(8,128)(2,1)S(1)}, bf16[288,128]{1,0:T(8,128)(2,1)S(1)}, u32[]{:S(2)}, u32[]{:S(2)}) collective-permute-start(bf16[288,128]{1,0:T(8,128)(2,1)S(1)} %get-tuple-element.31.refs_0_), channel_id=1, source_target_pairs={{0,64},{4,20},{8,72},{12,28},{16,80},{20,4},{24,88},{28,12},{32,96... | collective-permute-start | bytes 221192 | tf_op jit(solution)/shard_map/ppermute | solution.py:338
  27.8 4.4 %collective-permute-start.5 = (bf16[288,128]{1,0:T(8,128)(2,1)S(1)}, bf16[288,128]{1,0:T(8,128)(2,1)S(1)}, u32[]{:S(2)}, u32[]{:S(2)}) collective-permute-start(bf16[288,128]{1,0:T(8,128)(2,1)S(1)} %get-tuple-element.31.refs_0_), channel_id=1, source_target_pairs={{0,96},{4,28},{8,104},{12,4},{16,112},{20,12},{24,120},{28,20},{32... | collective-permute-start | bytes 221192 | tf_op jit(solution)/shard_map/ppermute | solution.py:338
  28.5 5.6 %collective-permute-start.4 = (bf16[288,128]{1,0:T(8,128)(2,1)S(1)}, bf16[288,128]{1,0:T(8,128)(2,1)S(1)}, u32[]{:S(2)}, u32[]{:S(2)}) collective-permute-start(bf16[288,128]{1,0:T(8,128)(2,1)S(1)} %get-tuple-element.31.refs_0_), channel_id=1, source_target_pairs={{0,32},{4,12},{8,40},{12,20},{16,48},{20,28},{24,56},{28,4},{32,64... | collective-permute-start | bytes 221192 | tf_op jit(solution)/shard_map/ppermute | solution.py:338
  34.1 11.4 %collective-permute-start.9 = (bf16[1248,128]{1,0:T(8,128)(2,1)S(1)}, bf16[1248,128]{1,0:T(8,128)(2,1)S(1)}, u32[]{:S(2)}, u32[]{:S(2)}) collective-permute-start(bf16[1248,128]{1,0:T(8,128)(2,1)S(1)} %shard_map.98.refs_0_.refs_1_.refs_7_), channel_id=1, source_target_pairs={{0,16},{4,68},{8,24},{12,76},{16,0},{20,84},{24,8},{28,92},{32,48}... | collective-permute-start | bytes 958472 | tf_op jit(solution)/shard_map/ppermute | solution.py:353
  40.5 5.6 %collective-permute-start.16 = (bf16[1248,128]{1,0:T(8,128)(2,1)S(1)}, bf16[1248,128]{1,0:T(8,128)(2,1)S(1)}, u32[]{:S(2)}, u32[]{:S(2)}) collective-permute-start(bf16[1248,128]{1,0:T(8,128)(2,1)S(1)} %shard_map.98.refs_0_.refs_1_.refs_7_), channel_id=1, source_target_pairs={{0,4},{4,0},{8,12},{12,8},{16,20},{20,16},{24,28},{28,24},{32,36},... | collective-permute-start | bytes 958472 | tf_op jit(solution)/shard_map/ppermute | solution.py:350
  40.5 9.1 %collective-permute-start.8 = (bf16[1248,128]{1,0:T(8,128)(2,1)S(1)}, bf16[1248,128]{1,0:T(8,128)(2,1)S(1)}, u32[]{:S(2)}, u32[]{:S(2)}) collective-permute-start(bf16[1248,128]{1,0:T(8,128)(2,1)S(1)} %shard_map.98.refs_0_.refs_1_.refs_7_), channel_id=1, source_target_pairs={{0,24},{4,100},{8,0},{12,108},{16,8},{20,116},{24,16},{28,124},{32... | collective-permute-start | bytes 958472 | tf_op jit(solution)/shard_map/ppermute | solution.py:353
  41.9 8.2 %collective-permute-start.7 = (bf16[1248,128]{1,0:T(8,128)(2,1)S(1)}, bf16[1248,128]{1,0:T(8,128)(2,1)S(1)}, u32[]{:S(2)}, u32[]{:S(2)}) collective-permute-start(bf16[1248,128]{1,0:T(8,128)(2,1)S(1)} %shard_map.98.refs_0_.refs_1_.refs_7_), channel_id=1, source_target_pairs={{0,8},{4,36},{8,16},{12,44},{16,24},{20,52},{24,0},{28,60},{32,40}... | collective-permute-start | bytes 958472 | tf_op jit(solution)/shard_map/ppermute | solution.py:353
  45.5 4.6 %collective-permute-start.19 = (bf16[1248,128]{1,0:T(8,128)(2,1)S(1)}, bf16[1248,128]{1,0:T(8,128)(2,1)S(1)}, u32[]{:S(2)}, u32[]{:S(2)}) collective-permute-start(bf16[1248,128]{1,0:T(8,128)(2,1)S(1)} %collective-permute-done.9.refs_3_.refs_4_.refs_10_), channel_id=1, source_target_pairs={{0,4},{4,0},{8,12},{12,8},{16,20},{20,16},{24,28},{28,24},{32,36},... | collective-permute-start | bytes 958472 | tf_op jit(solution)/shard_map/ppermute | solution.py:354
  45.5 19.5 %collective-permute-start.25 = (bf16[128,2048]{1,0:T(8,128)(2,1)S(1)}, bf16[128,2048]{1,0:T(8,128)(2,1)S(1)}, u32[]{:S(2)}, u32[]{:S(2)}) collective-permute-start(bf16[128,2048]{1,0:T(8,128)(2,1)S(1)} %get-tuple-element.48), channel_id=1, source_target_pairs={{0,2},{1,3},{2,0},{3,1},{4,6},{5,7},{6,4},{7,5},{8,10},{9,11},{10,... | collective-permute-start | bytes 1572872 | tf_op jit(solution)/shard_map/ppermute | solution.py:364
  46.1 24.2 %collective-permute-start.24 = (bf16[128,2048]{1,0:T(8,128)(2,1)S(1)}, bf16[128,2048]{1,0:T(8,128)(2,1)S(1)}, u32[]{:S(2)}, u32[]{:S(2)}) collective-permute-start(bf16[128,2048]{1,0:T(8,128)(2,1)S(1)} %get-tuple-element.48), channel_id=1, source_target_pairs={{0,3},{1,0},{2,1},{3,2},{4,7},{5,4},{6,5},{7,6},{8,11},{9,8},{10,9... | collective-permute-start | bytes 1572872 | tf_op jit(solution)/shard_map/ppermute | solution.py:364
  49.6 22.9 %collective-permute-start.23 = (bf16[128,2048]{1,0:T(8,128)(2,1)S(1)}, bf16[128,2048]{1,0:T(8,128)(2,1)S(1)}, u32[]{:S(2)}, u32[]{:S(2)}) collective-permute-start(bf16[128,2048]{1,0:T(8,128)(2,1)S(1)} %get-tuple-element.48), channel_id=1, source_target_pairs={{0,1},{1,2},{2,3},{3,0},{4,5},{5,6},{6,7},{7,4},{8,9},{9,10},{10,1... | collective-permute-start | bytes 1572872 | tf_op jit(solution)/shard_map/ppermute | solution.py:364
  50.1 9.4 %collective-permute-start.18 = (bf16[1248,128]{1,0:T(8,128)(2,1)S(1)}, bf16[1248,128]{1,0:T(8,128)(2,1)S(1)}, u32[]{:S(2)}, u32[]{:S(2)}) collective-permute-start(bf16[1248,128]{1,0:T(8,128)(2,1)S(1)} %collective-permute-done.8.refs_2_.refs_3_.refs_9_), channel_id=1, source_target_pairs={{0,4},{4,0},{8,12},{12,8},{16,20},{20,16},{24,28},{28,24},{32,36},... | collective-permute-start | bytes 958472 | tf_op jit(solution)/shard_map/ppermute | solution.py:354
  50.1 9.4 %collective-permute-start.17 = (bf16[1248,128]{1,0:T(8,128)(2,1)S(1)}, bf16[1248,128]{1,0:T(8,128)(2,1)S(1)}, u32[]{:S(2)}, u32[]{:S(2)}) collective-permute-start(bf16[1248,128]{1,0:T(8,128)(2,1)S(1)} %collective-permute-done.7.refs_1_.refs_2_.refs_8_), channel_id=1, source_target_pairs={{0,4},{4,0},{8,12},{12,8},{16,20},{20,16},{24,28},{28,24},{32,36},... | collective-permute-start | bytes 958472 | tf_op jit(solution)/shard_map/ppermute | solution.py:354
  72.6 110.9 %collective-permute-start.26 = (bf16[128,2048]{1,0:T(8,128)(2,1)S(1)}, bf16[128,2048]{1,0:T(8,128)(2,1)S(1)}, u32[]{:S(2)}, u32[]{:S(2)}) collective-permute-start(bf16[128,2048]{1,0:T(8,128)(2,1)S(1)} %collective-permute-done.23.w1), channel_id=1, source_target_pairs={{0,4},{4,0},{8,12},{12,8},{16,20},{20,16},{24,28},{28,24},{32,36},... | collective-permute-start | bytes 1572872 | tf_op jit(solution)/shard_map/ppermute | solution.py:374
  72.6 110.9 %collective-permute-start.27 = (bf16[128,2048]{1,0:T(8,128)(2,1)S(1)}, bf16[128,2048]{1,0:T(8,128)(2,1)S(1)}, u32[]{:S(2)}, u32[]{:S(2)}) collective-permute-start(bf16[128,2048]{1,0:T(8,128)(2,1)S(1)} %collective-permute-done.24.w2), channel_id=1, source_target_pairs={{0,4},{4,0},{8,12},{12,8},{16,20},{20,16},{24,28},{28,24},{32,36},... | collective-permute-start | bytes 1572872 | tf_op jit(solution)/shard_map/ppermute | solution.py:374
  73.1 110.4 %collective-permute-start.28 = (bf16[128,2048]{1,0:T(8,128)(2,1)S(1)}, bf16[128,2048]{1,0:T(8,128)(2,1)S(1)}, u32[]{:S(2)}, u32[]{:S(2)}) collective-permute-start(bf16[128,2048]{1,0:T(8,128)(2,1)S(1)} %collective-permute-done.25.w3), channel_id=1, source_target_pairs={{0,4},{4,0},{8,12},{12,8},{16,20},{20,16},{24,28},{28,24},{32,36},... | collective-permute-start | bytes 1572872 | tf_op jit(solution)/shard_map/ppermute | solution.py:374
  73.1 6.2 %collective-permute-start.12 = (bf16[384,128]{1,0:T(8,128)(2,1)S(1)}, bf16[384,128]{1,0:T(8,128)(2,1)S(1)}, u32[]{:S(2)}, u32[]{:S(2)}) collective-permute-start(bf16[384,128]{1,0:T(8,128)(2,1)S(1)} %shard_map.99), channel_id=1, source_target_pairs={{0,64},{4,20},{8,72},{12,28},{16,80},{20,4},{24,88},{28,12},{32,96... | collective-permute-start | bytes 294920 | tf_op jit(solution)/shard_map/ppermute | solution.py:358
  73.2 6.1 %collective-permute-start.11 = (bf16[384,128]{1,0:T(8,128)(2,1)S(1)}, bf16[384,128]{1,0:T(8,128)(2,1)S(1)}, u32[]{:S(2)}, u32[]{:S(2)}) collective-permute-start(bf16[384,128]{1,0:T(8,128)(2,1)S(1)} %shard_map.99), channel_id=1, source_target_pairs={{0,96},{4,28},{8,104},{12,4},{16,112},{20,12},{24,120},{28,20},{32... | collective-permute-start | bytes 294920 | tf_op jit(solution)/shard_map/ppermute | solution.py:358
  79.3 5.8 %collective-permute-start.10 = (bf16[384,128]{1,0:T(8,128)(2,1)S(1)}, bf16[384,128]{1,0:T(8,128)(2,1)S(1)}, u32[]{:S(2)}, u32[]{:S(2)}) collective-permute-start(bf16[384,128]{1,0:T(8,128)(2,1)S(1)} %shard_map.99), channel_id=1, source_target_pairs={{0,32},{4,12},{8,40},{12,20},{16,48},{20,28},{24,56},{28,4},{32,64... | collective-permute-start | bytes 294920 | tf_op jit(solution)/shard_map/ppermute | solution.py:358
  79.3 5.8 %collective-permute-start.15 = (bf16[384,128]{1,0:T(8,128)(2,1)S(1)}, bf16[384,128]{1,0:T(8,128)(2,1)S(1)}, u32[]{:S(2)}, u32[]{:S(2)}) collective-permute-start(bf16[384,128]{1,0:T(8,128)(2,1)S(1)} %collective-permute-done.12.refs_3_), channel_id=1, source_target_pairs={{0,4},{4,0},{8,12},{12,8},{16,20},{20,16},{24,28},{28,24},{32,36},... | collective-permute-start | bytes 294920 | tf_op jit(solution)/shard_map/ppermute | solution.py:359
  85.1 1.3 collective-permute-start.14
  85.1 1.5 collective-permute-start.13
  86.6 96.9 %copy-start.1 = (bf16[256,2048]{1,0:T(8,128)(2,1)S(1)}, bf16[256,2048]{1,0:T(8,128)(2,1)}, u32[]{:S(2)}) copy-start(bf16[256,2048]{1,0:T(8,128)(2,1)} %w0.1) | copy-start | bytes 3145732
  172.5 5.4 %collective-permute-start.20 = (bf16[96,256]{1,0:T(8,128)(2,1)S(1)}, bf16[96,256]{1,0:T(8,128)(2,1)S(1)}, u32[]{:S(2)}, u32[]{:S(2)}) collective-permute-start(bf16[96,256]{1,0:T(8,128)(2,1)S(1)} %get-tuple-element.44), channel_id=1, source_target_pairs={{0,1},{1,2},{2,3},{3,0},{4,5},{5,6},{6,7},{7,4},{8,9},{9,10},{10,1... | collective-permute-start | bytes 147464 | tf_op jit(solution)/shard_map/ppermute | solution.py:377
  172.6 5.3 %collective-permute-start.21 = (bf16[96,256]{1,0:T(8,128)(2,1)S(1)}, bf16[96,256]{1,0:T(8,128)(2,1)S(1)}, u32[]{:S(2)}, u32[]{:S(2)}) collective-permute-start(bf16[96,256]{1,0:T(8,128)(2,1)S(1)} %get-tuple-element.45), channel_id=1, source_target_pairs={{0,3},{1,0},{2,1},{3,2},{4,7},{5,4},{6,5},{7,6},{8,11},{9,8},{10,9... | collective-permute-start | bytes 147464 | tf_op jit(solution)/shard_map/ppermute | solution.py:377
  177.9 5.6 %collective-permute-start.22 = (bf16[96,256]{1,0:T(8,128)(2,1)S(1)}, bf16[96,256]{1,0:T(8,128)(2,1)S(1)}, u32[]{:S(2)}, u32[]{:S(2)}) collective-permute-start(bf16[96,256]{1,0:T(8,128)(2,1)S(1)} %get-tuple-element.46), channel_id=1, source_target_pairs={{0,2},{1,3},{2,0},{3,1},{4,6},{5,7},{6,4},{7,5},{8,10},{9,11},{10,... | collective-permute-start | bytes 147464 | tf_op jit(solution)/shard_map/ppermute | solution.py:377
where the time goes:
time: 187 us; the launch traced here: 186 us
  Pallas kernels  105 us (56%)
  waiting for transfers between devices  43.3 us (23%)
  starting transfers between devices  29.7 us (16%)
  local copies, waits for them, and re-layouts  5.39 us (3%)
    pallas_call x4, Pallas kernels, attend(): pl.pallas_call(functools.partial(attend_kernel, n_kv=len(kvs), n_extra=le...  100 us
    ppermute x3, waiting for transfers between devices, body(): rest.append(lax.ppermute(line_far, 'sp', grid_move(k, True)))  10.2 us
    ppermute x3, starting transfers between devices, body(): got.append(lax.ppermute(load, 'sp', grid_move(k, False)))  8.42 us
    ppermute x1, waiting for transfers between devices, body(): from_left = lax.ppermute(tokens, 'tp', ring(4, 1))  7.68 us
    ppermute x3, waiting for transfers between devices, body(): lax.ppermute(att[i], 'tp', ring(4, k))  7.65 us
    ppermute x3, waiting for transfers between devices, body(): rows_in.append(lax.ppermute(mine, 'tp', ring(4, k)))  7.53 us
    ppermute x3, starting transfers between devices, body(): line.append(lax.ppermute(kv_near, 'sp', grid_move(k, True)))  6.17 us
    ppermute x3, waiting for transfers between devices, body(): got.append(lax.ppermute(load, 'sp', grid_move(k, False)))  5.76 us
  transfers between devices with their start and end apart: 29, of which 14 were waited for; matrix products, arithmetic and copies ran while one was open for 1% of the time, Pallas kernels for 55%

commit v1 on v0

--- a/solution.py
+++ b/solution.py
@@ -44,11 +44,10 @@
 
 
 def angle_rows(sp, tp, n):
-    lane = lax.broadcasted_iota(jnp.int32, (64, 512), 1)
-    row = lax.broadcasted_iota(jnp.int32, (64, 512), 0)
-    again = lane >= 4 * n
-    block = jnp.where(again, 3, lax.div(lane, n))
-    inside = jnp.where(again, lane - 4 * n, lax.rem(lane, n))
+    lane = lax.broadcasted_iota(jnp.int32, (64, 4 * n), 1)
+    row = lax.broadcasted_iota(jnp.int32, (64, 4 * n), 0)
+    block = lax.div(lane, n)
+    inside = lax.rem(lane, n)
     shift = jnp.where(block == 0, 0, jnp.where(block == 1, 3, jnp.where(block == 2, 1, 2)))
     place = sp * (4 * n) + ((tp + shift) & 3) * n + inside
     freq = jnp.asarray(np.tile(ROPE_BASE ** (-np.arange(16) / 16.0), 4)[:, None], jnp.float32)
@@ -86,28 +85,24 @@
     wo_ref[...] = wo[pl.ds(pl.multiple_of(place[0] * half, half), half), :]
 
 
-def near_kernel(raw_own, t1, t2, weight, gk, tab, raw_ref, kv_ref, raw):
+def near_kernel(t1, t2, weight, raw_ref):
     n = t1.shape[0]
-    raw[3 * n :, :] = jnp.zeros((n, 128), jnp.bfloat16)
-    raw[:n, :] = raw_own[:, 256:]
-    raw_ref[:n, :] = raw_own[:, :256]
-    for i, t in ((1, t1), (2, t2)):
-        made = dot(t[...], weight[...]).astype(jnp.bfloat16)
-        raw[i * n : (i + 1) * n, :] = made[:, 256:]
-        raw_ref[i * n : (i + 1) * n, :] = made[:, :256]
-    kv_ref[...] = keys_values(raw[...], column(gk[...]), tab[:, : 4 * n])[: 3 * n]
-
-
-def far_kernel(t3, t4, rawq, weight, gq, gk, tab, qt_ref, kv_ref, raw, raw_far):
+    for i, t in enumerate((t1, t2)):
+        raw_ref[i * n : (i + 1) * n, :] = dot(t[...], weight[...]).astype(jnp.bfloat16)
+
+
+def far_kernel(t3, t4, raw_own, raw_near, weight, gk, tab, kv_ref, raw_ref, raw):
     n = 2 * t3.shape[0]
-    raw_far[n:, :] = jnp.zeros((128 - n, 128), jnp.bfloat16)
     made = dot(jnp.concatenate([t3[...], t4[...]], axis=0), weight[...]).astype(jnp.bfloat16)
-    raw_far[:n, :] = made[:, 256:]
-    kv_ref[...] = keys_values(raw_far[...], column(gk[...]), tab[:, 4 * n :])[:n]
-    raw[: 3 * n, :] = rawq[...]
-    raw[3 * n :, :] = made[:, :256]
-    table = tab[:, : 4 * n]
-    count = 4 * n
+    for at, part in ((0, raw_own[...]), (n, raw_near[...]), (3 * n, made)):
+        raw[at : at + part.shape[0], :] = part[:, 256:]
+        raw_ref[at : at + part.shape[0], :] = part[:, :256]
+    kv_ref[...] = keys_values(raw[...], column(gk[...]), tab[...])
+
+
+def query_kernel(raw, gq, tab, qt_ref):
+    count = raw.shape[0]
+    table = tab[...]
     for h in range(4):
         if h % 2 == 0:
             both = raw[:, h * 64 : h * 64 + 128].astype(jnp.float32).T
@@ -125,16 +120,13 @@
         at += p.shape[0]
 
 
-def join(parts, size=None):
-    size = size or parts[0].shape[0]
-    rows = [min(size, p.shape[0]) for p in parts]
-    specs = [pl.BlockSpec((r, 128), lambda i, b=p.shape[0] // r - 1: (b, 0)) for p, r in zip(parts, rows)]
+def join(parts):
+    rows = sum(p.shape[0] for p in parts)
     return pl.pallas_call(
         join_kernel,
-        grid=(1,),
-        out_shape=jax.ShapeDtypeStruct((sum(rows), 128), jnp.bfloat16),
-        in_specs=specs,
-        out_specs=pl.BlockSpec((sum(rows), 128), lambda i: (0, 0)),
+        out_shape=jax.ShapeDtypeStruct((rows, 128), jnp.bfloat16),
+        in_specs=[VMEM] * len(parts),
+        out_specs=VMEM,
         compiler_params=pltpu.CompilerParams(vmem_limit_bytes=4 * 2**20),
         cost_estimate=pl.CostEstimate(flops=1000, bytes_accessed=2**19, transcendentals=0),
     )(*parts)
@@ -278,14 +270,12 @@
     )(*args)
 
 
-def mix_kernel(place, lse, a0, a1, a2, a3, w0, w1, w2, w3, x1, x2, x3, out_ref, lse_ref):
+def early_kernel(place, lse, a0, w0, w1, w2, w3, x1, x2, x3, part_ref, rows_ref, lse_ref):
     half = w1.shape[0]
-    here = pl.ds(pl.multiple_of(place[0] * half, half), half)
-    there = pl.ds(pl.multiple_of((1 - place[0]) * half, half), half)
-    total = dot(a0[...], w0[...])
-    for a, w, x in ((a1, w1, x1), (a2, w2, x2), (a3, w3, x3)):
-        total += dot(a[:, here], w[...]) + dot(a[:, there], x[...])
-    out_ref[...] = total.astype(jnp.bfloat16)
+    part_ref[...] = dot(a0[...], w0[...])
+    for i, (w, x) in enumerate(((w1, x1), (w2, x2), (w3, x3))):
+        rows_ref[pl.ds(pl.multiple_of((2 * i + place[0]) * half, half), half), :] = w[...]
+        rows_ref[pl.ds(pl.multiple_of((2 * i + 1 - place[0]) * half, half), half), :] = x[...]
     n = lse.shape[1] // 4
     cyc = [lse[:, i * n : (i + 1) * n] for i in (0, 2, 3, 1)]
     for t in range(4):
@@ -293,6 +283,11 @@
         @pl.when(place[1] == t)
         def _():
             lse_ref[...] = jnp.concatenate([cyc[(a - t) % 4] for a in range(4)], axis=1)
+
+
+def mix_kernel(part, a1, a2, a3, rows, out_ref):
+    both = jnp.concatenate([a1[...], a2[...], a3[...]], axis=1)
+    out_ref[...] = (part[...] + dot(both, rows[...])).astype(jnp.bfloat16)
 
 
 def body(tokens, query_weight, key_weight, value_weight, out_weight, query_gain, key_gain):
@@ -324,65 +319,84 @@
         compiler_params=small,
         cost_estimate=cost(n),
     )(place, tokens, query_weight, key_weight.T, value_weight.T, out_weight)
-    rawq, kv_near = pl.pallas_call(
+    raw_near = pl.pallas_call(
         near_kernel,
-        out_shape=(jax.ShapeDtypeStruct((3 * n, 256), bf16), jax.ShapeDtypeStruct((3 * n, 128), bf16)),
-        in_specs=[VMEM] * 6,
+        out_shape=jax.ShapeDtypeStruct((2 * n, 384), bf16),
+        in_specs=[VMEM] * 3,
+        out_specs=VMEM,
+        compiler_params=small,
+        cost_estimate=cost(2 * n),
+    )(from_left, from_right, weight)
+    kv, raw = pl.pallas_call(
+        far_kernel,
+        out_shape=(jax.ShapeDtypeStruct((4 * n, 128), bf16), jax.ShapeDtypeStruct((4 * n, 256), bf16)),
+        in_specs=[VMEM] * 7,
         out_specs=(VMEM, VMEM),
         scratch_shapes=[pltpu.VMEM((4 * n, 128), bf16)],
         compiler_params=small,
-        cost_estimate=cost(3 * n),
-    )(raw_own, from_left, from_right, weight, key_gain, table)
-    line = [kv_near]
+        cost_estimate=cost(n),
+    )(far_a, far_b, raw_own, raw_near, weight, key_gain, table)
+    line = [kv]
     for k in (1, 3, 2):
-        line.append(lax.ppermute(kv_near, "sp", grid_move(k, True)))
-    qt, kv_far = pl.pallas_call(
-        far_kernel,
-        out_shape=(jax.ShapeDtypeStruct((128, 16 * n), bf16), jax.ShapeDtypeStruct((n, 128), bf16)),
-        in_specs=[VMEM] * 7,
-        out_specs=(VMEM, VMEM),
-        scratch_shapes=[pltpu.VMEM((4 * n, 256), bf16), pltpu.VMEM((128, 128), bf16)],
+        line.append(lax.ppermute(kv, "sp", grid_move(k, True)))
+    qt = pl.pallas_call(
+        query_kernel,
+        out_shape=jax.ShapeDtypeStruct((128, 16 * n), bf16),
+        in_specs=[VMEM] * 3,
+        out_specs=VMEM,
         compiler_params=small,
         cost_estimate=cost(n),
-    )(far_a, far_b, rawq, weight, query_gain, key_gain, table)
-
-    load = join([*line, kv_far])
-    twin = [lax.ppermute(load, "sp", core_swap())]
-    got = [load]
+    )(raw, query_gain, table)
+
+    load = join(line)
+    plane = []
     for k in (1, 3, 2):
-        got.append(lax.ppermute(load, "sp", grid_move(k, False)))
-    twin += [lax.ppermute(p, "sp", core_swap()) for p in got[1:]]
-    line_far = join(got, n)
-    rest = []
-    for k in (1, 3, 2):
-        rest.append(lax.ppermute(line_far, "sp", grid_move(k, True)))
-    twin_rest = [lax.ppermute(p, "sp", core_swap()) for p in rest]
-
-    mine, _ = lax.optimization_barrier((mine, kv_near))
+        plane.append(lax.ppermute(load, "sp", grid_move(k, False)))
+    load_twin = lax.ppermute(load, "sp", core_swap())
+    plane_twin = []
+    for k, p in zip((1, 3, 2), plane):
+        plane_twin.append(lax.ppermute(p, "sp", core_swap()))
+
+    mine, _ = lax.optimization_barrier((mine, kv))
     rows_in = []
     for k in (1, 3, 2):
         rows_in.append(lax.ppermute(mine, "tp", ring(4, k)))
 
-    def thirds(j):
-        return [((j, 384 * i, 384),) for i in range(3)]
-
-    tails = tuple((j, 1152, 96) for j in range(4))
-    state = attend(qt, [got[0], twin[0]], thirds(0) + thirds(1), [], None, False, scale)
-    state = attend(qt, got, thirds(1) + thirds(2) + thirds(3) + [tails], [], state, False, scale)
-    state = attend(qt, twin, thirds(1) + thirds(2) + thirds(3) + [tails], [], state, False, scale)
-    *rows_in, _ = lax.optimization_barrier((*rows_in, state[2]))
+    def quarters(j):
+        return [((j, 384 * i, 384),) for i in range(4)]
+
+    state = attend(qt, [load, load_twin], quarters(0) + quarters(1), [], None, False, scale)
+    state = attend(qt, plane, quarters(0) + quarters(1) + quarters(2), [], state, False, scale)
+    rows_in = lax.optimization_barrier((*rows_in, state[2]))[:3]
     rows_other = [lax.ppermute(w, "sp", core_swap()) for w in rows_in]
-    ends = [((j, 0, 384),) for j in range(6)]
-    *att, lse = attend(qt, rest + twin_rest, ends, got + twin, state, True, scale)
-    back = [lax.ppermute(att[i], "tp", ring(4, k)) for i, k in ((2, 1), (1, 3), (3, 2))]
-    return pl.pallas_call(
+    *att, lse = attend(
+        qt, plane_twin, quarters(0) + quarters(1) + quarters(2), [load, load_twin, *plane], state, True, scale
+    )
+    back = []
+    for i, k in ((2, 1), (1, 3), (3, 2)):
+        back.append(lax.ppermute(att[i], "tp", ring(4, k)))
+    wide = out_weight.shape[1]
+    part, rows, log_sums = pl.pallas_call(
+        early_kernel,
+        out_shape=(
+            jax.ShapeDtypeStruct((n, wide), jnp.float32),
+            jax.ShapeDtypeStruct((6 * half, wide), bf16),
+            jax.ShapeDtypeStruct((4, 4 * n), jnp.float32),
+        ),
+        in_specs=[pl.BlockSpec(memory_space=pltpu.SMEM)] + [VMEM] * 9,
+        out_specs=(VMEM,) * 3,
+        compiler_params=small,
+        cost_estimate=pl.CostEstimate(flops=2 * n * 256 * 2048, bytes_accessed=2**22, transcendentals=0),
+    )(place, lse, att[0], out_weight, *rows_in, *rows_other)
+    mixed = pl.pallas_call(
         mix_kernel,
-        out_shape=(jax.ShapeDtypeStruct((n, out_weight.shape[1]), bf16), jax.ShapeDtypeStruct((4, 4 * n), jnp.float32)),
-        in_specs=[pl.BlockSpec(memory_space=pltpu.SMEM)] + [VMEM] * 12,
-        out_specs=(VMEM, VMEM),
-        compiler_params=small,
-        cost_estimate=pl.CostEstimate(flops=2 * n * 1024 * 2048, bytes_accessed=2**22, transcendentals=0),
-    )(place, lse, att[0], *back, out_weight, *rows_in, *rows_other)
+        out_shape=jax.ShapeDtypeStruct((n, wide), bf16),
+        in_specs=[VMEM] * 5,
+        out_specs=VMEM,
+        compiler_params=small,
+        cost_estimate=pl.CostEstimate(flops=2 * n * 768 * 2048, bytes_accessed=2**22, transcendentals=0),
+    )(part, *back, rows)
+    return mixed, log_sums
 
 
 def solution(mesh):

time: 187 us -> 161 us (0.86)
  waiting for transfers between devices: 43.3 us -> 21.5 us
  starting transfers between devices: 29.7 us -> 27.4 us
    ppermute x19 -> x13, waiting for transfers between devices: 28.1 us -> 12.7 us  [the longest x3 4.92 us: body(): plane.append(lax.ppermute(load, 'sp', grid_move(k, False)))]
    ppermute x1, waiting for transfers between devices: 7.68 us -> 2.44 us  [body(): from_left = lax.ppermute(tokens, 'tp', ring(4, 1))]
    ppermute x19 -> x13, starting transfers between devices: 20.7 us -> 16.4 us  [the longest x3 6.26 us: body(): line.append(lax.ppermute(kv, 'sp', grid_move(k, True)))]
    ppermute x3, waiting for transfers between devices: 7.53 us -> 3.96 us  [body(): rows_in.append(lax.ppermute(mine, 'tp', ring(4, k)))]
    ppermute x1, waiting for transfers between devices: 0.01 us -> 2.45 us  [body(): far_a = lax.ppermute(from_left[:n // 2], 'tp', ring(4, 1))]
    ppermute x3, starting transfers between devices: 1.76 us -> 3.74 us  [body(): rows_in.append(lax.ppermute(mine, 'tp', ring(4, k)))]
    pallas_call x4 -> x3, Pallas kernels: 100 us -> 99.4 us  [attend(): pl.pallas_call(functools.partial(attend_kernel, n_kv=len(kvs), n_extra=le...]
    pallas_call x5 -> x6, Pallas kernels: 3.83 us -> 4.61 us  [the longest x1 1.65 us: body(): pl.pallas_call(early_kernel, out_shape=(jax.ShapeDtypeStruct((n, wide), j...]
  transfers between devices with their start and end apart: 29 -> 23, of which waited for: 14 -> 10; matrix products, arithmetic and copies ran while one was open for 1% -> 0% of each run, Pallas kernels for 55% -> 64%
where the time goes in v1:
time: 161 us
  Pallas kernels  105 us (65%)
  starting transfers between devices  27.4 us (17%)
  waiting for transfers between devices  21.5 us (13%)
  local copies, waits for them, and re-layouts  5.39 us (3%)
    pallas_call x3, Pallas kernels, attend(): pl.pallas_call(functools.partial(attend_kernel, n_kv=len(kvs), n_extra=le...  99.4 us
    ppermute x3, starting transfers between devices, body(): line.append(lax.ppermute(kv, 'sp', grid_move(k, True)))  6.26 us
    unnamed x18, local copies, waits for them, and re-layouts  5.37 us
    ppermute x3, starting transfers between devices, body(): plane.append(lax.ppermute(load, 'sp', grid_move(k, False)))  5.3 us
    ppermute x3, waiting for transfers between devices, body(): plane.append(lax.ppermute(load, 'sp', grid_move(k, False)))  4.92 us
    ppermute x3, waiting for transfers between devices, body(): line.append(lax.ppermute(kv, 'sp', grid_move(k, True)))  4.51 us
    ppermute x3, starting transfers between devices, body(): back.append(lax.ppermute(att[i], 'tp', ring(4, k)))  4.01 us
    ppermute x3, waiting for transfers between devices, body(): rows_in.append(lax.ppermute(mine, 'tp', ring(4, k)))  3.96 us
  transfers between devices with their start and end apart: 23, of which 10 were waited for; matrix products, arithmetic and copies ran while one was open for 0% of the time, Pallas kernels for 64%

profile of v1, /device:TPU:0, one launch (start us, length us, event | category | flops | bytes accessed | tf_op | source)
XLA Modules:
  0.0 160.7 jit_solution(16847991955819583842)
XLA Ops:
  0.6 0.0 copy-start.8
  0.6 1.7 %collective-permute-start = (bf16[96,2048]{1,0:T(8,128)(2,1)}, bf16[96,2048]{1,0:T(8,128)(2,1)S(1)}, u32[]{:S(2)}, u32[]{:S(2)}) collective-permute-start(bf16[96,2048]{1,0:T(8,128)(2,1)} %t0.1), channel_id=1, source_target_pairs={{0,1},{1,2},{2,3},{3,0},{4,5},{5,6},{6,7},{7,4},{8,9},{9,10},{10,1... | collective-permute-start | bytes 1179656 | tf_op jit(solution)/shard_map/ppermute | solution.py:304
  2.3 1.6 %collective-permute-start.2 = (bf16[96,2048]{1,0:T(8,128)(2,1)}, bf16[96,2048]{1,0:T(8,128)(2,1)S(1)}, u32[]{:S(2)}, u32[]{:S(2)}) collective-permute-start(bf16[96,2048]{1,0:T(8,128)(2,1)} %t0.1), channel_id=1, source_target_pairs={{0,3},{1,0},{2,1},{3,2},{4,7},{5,4},{6,5},{7,6},{8,11},{9,8},{10,9... | collective-permute-start | bytes 1179656 | tf_op jit(solution)/shard_map/ppermute | solution.py:305
  3.9 0.1 pad_add_fusion.place
  4.0 1.2 copy-done
  5.2 1.2 copy-done.2
  6.5 1.0 copy-done.3
  7.5 0.9 copy-done.4
  8.4 0.9 copy-done.5
  9.4 1.1 shard_map.95
  10.5 2.4 %collective-permute-done.t1 = bf16[96,2048]{1,0:T(8,128)(2,1)S(1)} collective-permute-done((bf16[96,2048]{1,0:T(8,128)(2,1)}, bf16[96,2048]{1,0:T(8,128)(2,1)S(1)}, u32[]{:S(2)}, u32[]{:S(2)}) %collective-permute-start) | collective-permute-done | bytes 393248 | tf_op jit(solution)/shard_map/ppermute | solution.py:304
  12.9 0.0 copy-start.6
  12.9 0.5 collective-permute-start.1
  13.5 0.0 collective-permute-done.2.t2
  13.5 2.8 %collective-permute-start.3 = (bf16[48,2048]{1,0:T(8,128)(2,1)S(1)}, bf16[48,2048]{1,0:T(8,128)(2,1)S(1)}, u32[]{:S(2)}, u32[]{:S(2)}) collective-permute-start(bf16[48,2048]{1,0:T(8,128)(2,1)S(1)} %slice.9), channel_id=1, source_target_pairs={{0,3},{1,0},{2,1},{3,2},{4,7},{5,4},{6,5},{7,6},{8,11},{9,8},{10,9... | collective-permute-start | bytes 589832 | tf_op jit(solution)/shard_map/ppermute | solution.py:307
  16.3 0.4 sine_select_fusion.tab
  16.8 0.7 shard_map.96.raw_near
  17.5 2.5 %collective-permute-done.1.t3 = bf16[48,2048]{1,0:T(8,128)(2,1)S(1)} collective-permute-done((bf16[48,2048]{1,0:T(8,128)(2,1)S(1)}, bf16[48,2048]{1,0:T(8,128)(2,1)S(1)}, u32[]{:S(2)}, u32[]{:S(2)}) %collective-permute-start.1) | collective-permute-done | bytes 196640 | tf_op jit(solution)/shard_map/ppermute | solution.py:306
  19.9 0.0 collective-permute-done.3.t4
  19.9 0.6 shard_map.97
  20.5 4.2 %collective-permute-start.6 = (bf16[384,128]{1,0:T(8,128)(2,1)S(1)}, bf16[384,128]{1,0:T(8,128)(2,1)S(1)}, u32[]{:S(2)}, u32[]{:S(2)}) collective-permute-start(bf16[384,128]{1,0:T(8,128)(2,1)S(1)} %get-tuple-element.28.refs_0_), channel_id=1, source_target_pairs={{0,64},{4,20},{8,72},{12,28},{16,80},{20,4},{24,88},{28,12},{32,96... | collective-permute-start | bytes 294920 | tf_op jit(solution)/shard_map/ppermute | solution.py:341
  24.8 0.7 collective-permute-start.5
  25.5 1.3 collective-permute-start.4
  26.8 0.6 collective-permute-done.6.refs_3_
  27.4 2.1 %collective-permute-done.5.refs_2_ = bf16[384,128]{1,0:T(8,128)(2,1)S(1)} collective-permute-done((bf16[384,128]{1,0:T(8,128)(2,1)S(1)}, bf16[384,128]{1,0:T(8,128)(2,1)S(1)}, u32[]{:S(2)}, u32[]{:S(2)}) %collective-permute-start.5) | collective-permute-done | bytes 98336 | tf_op jit(solution)/shard_map/ppermute | solution.py:341
  29.4 1.9 %collective-permute-done.4.refs_1_ = bf16[384,128]{1,0:T(8,128)(2,1)S(1)} collective-permute-done((bf16[384,128]{1,0:T(8,128)(2,1)S(1)}, bf16[384,128]{1,0:T(8,128)(2,1)S(1)}, u32[]{:S(2)}, u32[]{:S(2)}) %collective-permute-start.4) | collective-permute-done | bytes 98336 | tf_op jit(solution)/shard_map/ppermute | solution.py:341
  31.3 0.1 collective-permute-start.13
  31.4 3.3 %collective-permute-start.11 = (bf16[1536,128]{1,0:T(8,128)(2,1)S(1)}, bf16[1536,128]{1,0:T(8,128)(2,1)S(1)}, u32[]{:S(2)}, u32[]{:S(2)}) collective-permute-start(bf16[1536,128]{1,0:T(8,128)(2,1)S(1)} %shard_map.99.refs_1_.refs_4_), channel_id=1, source_target_pairs={{0,16},{4,68},{8,24},{12,76},{16,0},{20,84},{24,8},{28,92},{32,48}... | collective-permute-start | bytes 1179656 | tf_op jit(solution)/shard_map/ppermute | solution.py:354
  34.7 1.1 collective-permute-start.9
  35.8 1.8 %collective-permute-start.16 = (bf16[128,2048]{1,0:T(8,128)(2,1)S(1)}, bf16[128,2048]{1,0:T(8,128)(2,1)S(1)}, u32[]{:S(2)}, u32[]{:S(2)}) collective-permute-start(bf16[128,2048]{1,0:T(8,128)(2,1)S(1)} %get-tuple-element.38), channel_id=1, source_target_pairs={{0,2},{1,3},{2,0},{3,1},{4,6},{5,7},{6,4},{7,5},{8,10},{9,11},{10,... | collective-permute-start | bytes 1572872 | tf_op jit(solution)/shard_map/ppermute | solution.py:363
  37.5 1.0 collective-permute-start.7
  38.5 0.0 collective-permute-done.13.refs_2_.refs_5_
  38.5 1.4 collective-permute-start.15
  39.9 0.8 collective-permute-done.11.refs_3_.refs_8_
  40.8 0.5 collective-permute-start.14
  41.3 4.1 %collective-permute-done.9.refs_2_.refs_7_ = bf16[1536,128]{1,0:T(8,128)(2,1)S(1)} collective-permute-done((bf16[1536,128]{1,0:T(8,128)(2,1)S(1)}, bf16[1536,128]{1,0:T(8,128)(2,1)S(1)}, u32[]{:S(2)}, u32[]{:S(2)}) %collective-permute-start.9) | collective-permute-done | bytes 393248 | tf_op jit(solution)/shard_map/ppermute | solution.py:354
  45.4 0.0 collective-permute-start.12
  45.4 0.2 shard_map.98.refs_0_
  45.6 4.6 %shard_map.100 = (f32[64,1536]{1,0:T(8,128)S(1)}, f32[8,1536]{1,0:T(8,128)S(1)}, f32[1,1536]{1,0:T(1,128)S(1)}) custom-call(bf16[128,1536]{1,0:T(8,128)(2,1)S(1)} %shard_map.98.refs_0_, bf16[1536,128]{1,0:T(8,128)(2,1)S(1)} %shard_map.99.refs_1_.refs_4_, bf16[1536,128]{1,0:T(8,128)(2,1)S(1)} %collective-permute-done.13.refs_2_.refs_5_), custom_call_target="tpu_custom_call" | custom-call | flops 1207959552 | bytes 1572864 | tf_op jit(solution)/shard_map/pallas_call | solution.py:257
  50.3 0.0 collective-permute-done.7.refs_1_.refs_6_
  50.3 0.8 collective-permute-start.10
  51.1 1.0 collective-permute-done.16.w3
  52.1 0.0 collective-permute-start.8
  52.1 6.3 %shard_map.101 = (f32[64,1536]{1,0:T(8,128)S(1)}, f32[8,1536]{1,0:T(8,128)S(1)}, f32[1,1536]{1,0:T(1,128)S(1)}) custom-call(bf16[128,1536]{1,0:T(8,128)(2,1)S(1)} %shard_map.98.refs_0_, bf16[1536,128]{1,0:T(8,128)(2,1)S(1)} %collective-permute-done.7.refs_1_.refs_6_, bf16[1536,128]{1,0:T(8,128)(2,1)S(1)} %collective-permute-done.9.refs_2_.refs_7_, ...), custom_call_target="tpu_custom_call" | custom-call | flops 1811939328 | bytes 1966080 | tf_op jit(solution)/shard_map/pallas_call | solution.py:257
  58.4 2.9 %collective-permute-done.15.w2 = bf16[128,2048]{1,0:T(8,128)(2,1)S(1)} collective-permute-done((bf16[128,2048]{1,0:T(8,128)(2,1)S(1)}, bf16[128,2048]{1,0:T(8,128)(2,1)S(1)}, u32[]{:S(2)}, u32[]{:S(2)}) %collective-permute-start.15) | collective-permute-done | bytes 524320 | tf_op jit(solution)/shard_map/ppermute | solution.py:363
  61.3 0.0 collective-permute-done.14.w1
  61.3 0.0 collective-permute-start.17
  61.3 0.5 collective-permute-start.18
  61.8 0.0 collective-permute-done.12.refs_3_
  61.8 0.0 collective-permute-start.19
  61.8 0.0 collective-permute-done.10.refs_2_
  61.8 0.0 collective-permute-done.8.refs_1_
  61.8 0.0 copy-start.1
  61.8 88.5 %shard_map.102 = (bf16[96,256]{1,0:T(8,128)(2,1)S(1)}, bf16[96,256]{1,0:T(8,128)(2,1)S(1)}, bf16[96,256]{1,0:T(8,128)(2,1)S(1)}, bf16[96,256]{1,0:T(8,128)(2,1)S(1)}, f32[4,384]{1,0:T(4,128)S(1)}) custom-call(bf16[128,1536]{1,0:T(8,128)(2,1)S(1)} %shard_map.98.refs_0_, bf16[1536,128]{1,0:T(8,128)(2,1)S(1)} %collective-permute-done.8.refs_1_, ...), custom_call_target="tpu_custom_call" | custom-call | flops 1811939328 | bytes 1966080 | tf_op jit(solution)/shard_map/pallas_call | solution.py:257
  150.3 0.3 collective-permute-start.20
  150.6 3.0 %collective-permute-start.21 = (bf16[96,256]{1,0:T(8,128)(2,1)S(1)}, bf16[96,256]{1,0:T(8,128)(2,1)S(1)}, u32[]{:S(2)}, u32[]{:S(2)}) collective-permute-start(bf16[96,256]{1,0:T(8,128)(2,1)S(1)} %get-tuple-element.44), channel_id=1, source_target_pairs={{0,3},{1,0},{2,1},{3,2},{4,7},{5,4},{6,5},{7,6},{8,11},{9,8},{10,9... | collective-permute-start | bytes 147464 | tf_op jit(solution)/shard_map/ppermute | solution.py:377
  153.6 0.0 collective-permute-done.17.x1
  153.6 0.7 collective-permute-start.22
  154.3 0.0 collective-permute-done.18.x2
  154.3 0.0 collective-permute-done.19.x3
  154.4 1.7 %shard_map.103 = (f32[96,2048]{1,0:T(8,128)S(1)}, bf16[768,2048]{1,0:T(8,128)(2,1)S(1)}, f32[4,384]{1,0:T(4,128)}) custom-call(s32[2]{0:T(128)S(1)} %pad_add_fusion.place, f32[4,384]{1,0:T(4,128)S(1)} %get-tuple-element.35.lse, bf16[96,256]{1,0:T(8,128)(2,1)S(1)} %get-tuple-element.36.a0, bf16[256,2048]{1,0:T(8,128)(2,1)S(1)} %copy-done.1, ...), custom_call_target="tpu_custom_call" | custom-call | flops 100663296 | bytes 4194304 | tf_op jit(solution)/shard_map/pallas_call | solution.py:379
  156.0 0.0 collective-permute-done.20.a1
  156.0 3.2 %collective-permute-done.22.a3 = bf16[96,256]{1,0:T(8,128)(2,1)S(1)} collective-permute-done((bf16[96,256]{1,0:T(8,128)(2,1)S(1)}, bf16[96,256]{1,0:T(8,128)(2,1)S(1)}, u32[]{:S(2)}, u32[]{:S(2)}) %collective-permute-start.22) | collective-permute-done | bytes 49184 | tf_op jit(solution)/shard_map/ppermute | solution.py:377
  159.2 1.4 shard_map.104
  (17 shorter events, 0.1 us)
Async XLA Ops:
  0.6 15.7 %copy-start.8 = (f32[64]{0:T(128)S(1)}, f32[64]{0:T(128)}, u32[]{:S(2)}) copy-start(f32[64]{0:T(128)} %constant.38) | copy-start | bytes 772
  0.6 12.3 %collective-permute-start = (bf16[96,2048]{1,0:T(8,128)(2,1)}, bf16[96,2048]{1,0:T(8,128)(2,1)S(1)}, u32[]{:S(2)}, u32[]{:S(2)}) collective-permute-start(bf16[96,2048]{1,0:T(8,128)(2,1)} %t0.1), channel_id=1, source_target_pairs={{0,1},{1,2},{2,3},{3,0},{4,5},{5,6},{6,7},{7,4},{8,9},{9,10},{10,1... | collective-permute-start | bytes 1179656 | tf_op jit(solution)/shard_map/ppermute | solution.py:304
  2.3 11.2 %collective-permute-start.2 = (bf16[96,2048]{1,0:T(8,128)(2,1)}, bf16[96,2048]{1,0:T(8,128)(2,1)S(1)}, u32[]{:S(2)}, u32[]{:S(2)}) collective-permute-start(bf16[96,2048]{1,0:T(8,128)(2,1)} %t0.1), channel_id=1, source_target_pairs={{0,3},{1,0},{2,1},{3,2},{4,7},{5,4},{6,5},{7,6},{8,11},{9,8},{10,9... | collective-permute-start | bytes 1179656 | tf_op jit(solution)/shard_map/ppermute | solution.py:305
  4.0 1.2 copy-start
  5.2 1.2 copy-start.2
  6.5 1.0 copy-start.3
  7.5 0.9 copy-start.4
  8.4 0.9 copy-start.5
  9.4 10.6 %copy-start.7 = (bf16[1,64]{1,0:T(2,128)(2,1)S(1)}, bf16[1,64]{1,0:T(2,128)(2,1)}, u32[]{:S(2)}) copy-start(bf16[1,64]{1,0:T(2,128)(2,1)} %gk.1) | copy-start | bytes 388
  12.9 32.5 %copy-start.6 = (bf16[4,64]{1,0:T(4,128)(2,1)S(1)}, bf16[4,64]{1,0:T(4,128)(2,1)}, u32[]{:S(2)}) copy-start(bf16[4,64]{1,0:T(4,128)(2,1)} %gq.1) | copy-start | bytes 1540
  12.9 7.0 %collective-permute-start.1 = (bf16[48,2048]{1,0:T(8,128)(2,1)S(1)}, bf16[48,2048]{1,0:T(8,128)(2,1)S(1)}, u32[]{:S(2)}, u32[]{:S(2)}) collective-permute-start(bf16[48,2048]{1,0:T(8,128)(2,1)S(1)} %slice.8), channel_id=1, source_target_pairs={{0,1},{1,2},{2,3},{3,0},{4,5},{5,6},{6,7},{7,4},{8,9},{9,10},{10,1... | collective-permute-start | bytes 589832 | tf_op jit(solution)/shard_map/ppermute | solution.py:306
  13.5 6.4 %collective-permute-start.3 = (bf16[48,2048]{1,0:T(8,128)(2,1)S(1)}, bf16[48,2048]{1,0:T(8,128)(2,1)S(1)}, u32[]{:S(2)}, u32[]{:S(2)}) collective-permute-start(bf16[48,2048]{1,0:T(8,128)(2,1)S(1)} %slice.9), channel_id=1, source_target_pairs={{0,3},{1,0},{2,1},{3,2},{4,7},{5,4},{6,5},{7,6},{8,11},{9,8},{10,9... | collective-permute-start | bytes 589832 | tf_op jit(solution)/shard_map/ppermute | solution.py:307
  20.5 6.8 %collective-permute-start.6 = (bf16[384,128]{1,0:T(8,128)(2,1)S(1)}, bf16[384,128]{1,0:T(8,128)(2,1)S(1)}, u32[]{:S(2)}, u32[]{:S(2)}) collective-permute-start(bf16[384,128]{1,0:T(8,128)(2,1)S(1)} %get-tuple-element.28.refs_0_), channel_id=1, source_target_pairs={{0,64},{4,20},{8,72},{12,28},{16,80},{20,4},{24,88},{28,12},{32,96... | collective-permute-start | bytes 294920 | tf_op jit(solution)/shard_map/ppermute | solution.py:341
  24.8 4.7 %collective-permute-start.5 = (bf16[384,128]{1,0:T(8,128)(2,1)S(1)}, bf16[384,128]{1,0:T(8,128)(2,1)S(1)}, u32[]{:S(2)}, u32[]{:S(2)}) collective-permute-start(bf16[384,128]{1,0:T(8,128)(2,1)S(1)} %get-tuple-element.28.refs_0_), channel_id=1, source_target_pairs={{0,96},{4,28},{8,104},{12,4},{16,112},{20,12},{24,120},{28,20},{32... | collective-permute-start | bytes 294920 | tf_op jit(solution)/shard_map/ppermute | solution.py:341
  25.5 5.8 %collective-permute-start.4 = (bf16[384,128]{1,0:T(8,128)(2,1)S(1)}, bf16[384,128]{1,0:T(8,128)(2,1)S(1)}, u32[]{:S(2)}, u32[]{:S(2)}) collective-permute-start(bf16[384,128]{1,0:T(8,128)(2,1)S(1)} %get-tuple-element.28.refs_0_), channel_id=1, source_target_pairs={{0,32},{4,12},{8,40},{12,20},{16,48},{20,28},{24,56},{28,4},{32,64... | collective-permute-start | bytes 294920 | tf_op jit(solution)/shard_map/ppermute | solution.py:341
  31.3 7.2 %collective-permute-start.13 = (bf16[1536,128]{1,0:T(8,128)(2,1)S(1)}, bf16[1536,128]{1,0:T(8,128)(2,1)S(1)}, u32[]{:S(2)}, u32[]{:S(2)}) collective-permute-start(bf16[1536,128]{1,0:T(8,128)(2,1)S(1)} %shard_map.99.refs_1_.refs_4_), channel_id=1, source_target_pairs={{0,4},{4,0},{8,12},{12,8},{16,20},{20,16},{24,28},{28,24},{32,36},... | collective-permute-start | bytes 1179656 | tf_op jit(solution)/shard_map/ppermute | solution.py:355
  31.4 9.4 %collective-permute-start.11 = (bf16[1536,128]{1,0:T(8,128)(2,1)S(1)}, bf16[1536,128]{1,0:T(8,128)(2,1)S(1)}, u32[]{:S(2)}, u32[]{:S(2)}) collective-permute-start(bf16[1536,128]{1,0:T(8,128)(2,1)S(1)} %shard_map.99.refs_1_.refs_4_), channel_id=1, source_target_pairs={{0,16},{4,68},{8,24},{12,76},{16,0},{20,84},{24,8},{28,92},{32,48}... | collective-permute-start | bytes 1179656 | tf_op jit(solution)/shard_map/ppermute | solution.py:354
  34.7 10.7 %collective-permute-start.9 = (bf16[1536,128]{1,0:T(8,128)(2,1)S(1)}, bf16[1536,128]{1,0:T(8,128)(2,1)S(1)}, u32[]{:S(2)}, u32[]{:S(2)}) collective-permute-start(bf16[1536,128]{1,0:T(8,128)(2,1)S(1)} %shard_map.99.refs_1_.refs_4_), channel_id=1, source_target_pairs={{0,24},{4,100},{8,0},{12,108},{16,8},{20,116},{24,16},{28,124},{32... | collective-permute-start | bytes 1179656 | tf_op jit(solution)/shard_map/ppermute | solution.py:354
  35.8 16.3 %collective-permute-start.16 = (bf16[128,2048]{1,0:T(8,128)(2,1)S(1)}, bf16[128,2048]{1,0:T(8,128)(2,1)S(1)}, u32[]{:S(2)}, u32[]{:S(2)}) collective-permute-start(bf16[128,2048]{1,0:T(8,128)(2,1)S(1)} %get-tuple-element.38), channel_id=1, source_target_pairs={{0,2},{1,3},{2,0},{3,1},{4,6},{5,7},{6,4},{7,5},{8,10},{9,11},{10,... | collective-permute-start | bytes 1572872 | tf_op jit(solution)/shard_map/ppermute | solution.py:363
  37.5 12.8 %collective-permute-start.7 = (bf16[1536,128]{1,0:T(8,128)(2,1)S(1)}, bf16[1536,128]{1,0:T(8,128)(2,1)S(1)}, u32[]{:S(2)}, u32[]{:S(2)}) collective-permute-start(bf16[1536,128]{1,0:T(8,128)(2,1)S(1)} %shard_map.99.refs_1_.refs_4_), channel_id=1, source_target_pairs={{0,8},{4,36},{8,16},{12,44},{16,24},{20,52},{24,0},{28,60},{32,40}... | collective-permute-start | bytes 1179656 | tf_op jit(solution)/shard_map/ppermute | solution.py:354
  38.5 22.8 %collective-permute-start.15 = (bf16[128,2048]{1,0:T(8,128)(2,1)S(1)}, bf16[128,2048]{1,0:T(8,128)(2,1)S(1)}, u32[]{:S(2)}, u32[]{:S(2)}) collective-permute-start(bf16[128,2048]{1,0:T(8,128)(2,1)S(1)} %get-tuple-element.38), channel_id=1, source_target_pairs={{0,3},{1,0},{2,1},{3,2},{4,7},{5,4},{6,5},{7,6},{8,11},{9,8},{10,9... | collective-permute-start | bytes 1572872 | tf_op jit(solution)/shard_map/ppermute | solution.py:363
  40.8 20.5 %collective-permute-start.14 = (bf16[128,2048]{1,0:T(8,128)(2,1)S(1)}, bf16[128,2048]{1,0:T(8,128)(2,1)S(1)}, u32[]{:S(2)}, u32[]{:S(2)}) collective-permute-start(bf16[128,2048]{1,0:T(8,128)(2,1)S(1)} %get-tuple-element.38), channel_id=1, source_target_pairs={{0,1},{1,2},{2,3},{3,0},{4,5},{5,6},{6,7},{7,4},{8,9},{9,10},{10,1... | collective-permute-start | bytes 1572872 | tf_op jit(solution)/shard_map/ppermute | solution.py:363
  45.4 16.4 %collective-permute-start.12 = (bf16[1536,128]{1,0:T(8,128)(2,1)S(1)}, bf16[1536,128]{1,0:T(8,128)(2,1)S(1)}, u32[]{:S(2)}, u32[]{:S(2)}) collective-permute-start(bf16[1536,128]{1,0:T(8,128)(2,1)S(1)} %collective-permute-done.11.refs_3_.refs_8_), channel_id=1, source_target_pairs={{0,4},{4,0},{8,12},{12,8},{16,20},{20,16},{24,28},{28,24},{32,36},... | collective-permute-start | bytes 1179656 | tf_op jit(solution)/shard_map/ppermute | solution.py:358
  50.3 11.5 %collective-permute-start.10 = (bf16[1536,128]{1,0:T(8,128)(2,1)S(1)}, bf16[1536,128]{1,0:T(8,128)(2,1)S(1)}, u32[]{:S(2)}, u32[]{:S(2)}) collective-permute-start(bf16[1536,128]{1,0:T(8,128)(2,1)S(1)} %collective-permute-done.9.refs_2_.refs_7_), channel_id=1, source_target_pairs={{0,4},{4,0},{8,12},{12,8},{16,20},{20,16},{24,28},{28,24},{32,36},... | collective-permute-start | bytes 1179656 | tf_op jit(solution)/shard_map/ppermute | solution.py:358
  52.1 9.7 %collective-permute-start.8 = (bf16[1536,128]{1,0:T(8,128)(2,1)S(1)}, bf16[1536,128]{1,0:T(8,128)(2,1)S(1)}, u32[]{:S(2)}, u32[]{:S(2)}) collective-permute-start(bf16[1536,128]{1,0:T(8,128)(2,1)S(1)} %collective-permute-done.7.refs_1_.refs_6_), channel_id=1, source_target_pairs={{0,4},{4,0},{8,12},{12,8},{16,20},{20,16},{24,28},{28,24},{32,36},... | collective-permute-start | bytes 1179656 | tf_op jit(solution)/shard_map/ppermute | solution.py:358
  61.3 92.4 %collective-permute-start.17 = (bf16[128,2048]{1,0:T(8,128)(2,1)S(1)}, bf16[128,2048]{1,0:T(8,128)(2,1)S(1)}, u32[]{:S(2)}, u32[]{:S(2)}) collective-permute-start(bf16[128,2048]{1,0:T(8,128)(2,1)S(1)} %collective-permute-done.14.w1), channel_id=1, source_target_pairs={{0,4},{4,0},{8,12},{12,8},{16,20},{20,16},{24,28},{28,24},{32,36},... | collective-permute-start | bytes 1572872 | tf_op jit(solution)/shard_map/ppermute | solution.py:371
  61.3 93.1 %collective-permute-start.18 = (bf16[128,2048]{1,0:T(8,128)(2,1)S(1)}, bf16[128,2048]{1,0:T(8,128)(2,1)S(1)}, u32[]{:S(2)}, u32[]{:S(2)}) collective-permute-start(bf16[128,2048]{1,0:T(8,128)(2,1)S(1)} %collective-permute-done.15.w2), channel_id=1, source_target_pairs={{0,4},{4,0},{8,12},{12,8},{16,20},{20,16},{24,28},{28,24},{32,36},... | collective-permute-start | bytes 1572872 | tf_op jit(solution)/shard_map/ppermute | solution.py:371
  61.8 92.6 %collective-permute-start.19 = (bf16[128,2048]{1,0:T(8,128)(2,1)S(1)}, bf16[128,2048]{1,0:T(8,128)(2,1)S(1)}, u32[]{:S(2)}, u32[]{:S(2)}) collective-permute-start(bf16[128,2048]{1,0:T(8,128)(2,1)S(1)} %collective-permute-done.16.w3), channel_id=1, source_target_pairs={{0,4},{4,0},{8,12},{12,8},{16,20},{20,16},{24,28},{28,24},{32,36},... | collective-permute-start | bytes 1572872 | tf_op jit(solution)/shard_map/ppermute | solution.py:371
  61.8 92.5 %copy-start.1 = (bf16[256,2048]{1,0:T(8,128)(2,1)S(1)}, bf16[256,2048]{1,0:T(8,128)(2,1)}, u32[]{:S(2)}) copy-start(bf16[256,2048]{1,0:T(8,128)(2,1)} %w0.1) | copy-start | bytes 3145732
  150.3 5.7 %collective-permute-start.20 = (bf16[96,256]{1,0:T(8,128)(2,1)S(1)}, bf16[96,256]{1,0:T(8,128)(2,1)S(1)}, u32[]{:S(2)}, u32[]{:S(2)}) collective-permute-start(bf16[96,256]{1,0:T(8,128)(2,1)S(1)} %get-tuple-element.43), channel_id=1, source_target_pairs={{0,1},{1,2},{2,3},{3,0},{4,5},{5,6},{6,7},{7,4},{8,9},{9,10},{10,1... | collective-permute-start | bytes 147464 | tf_op jit(solution)/shard_map/ppermute | solution.py:377
  150.6 5.4 %collective-permute-start.21 = (bf16[96,256]{1,0:T(8,128)(2,1)S(1)}, bf16[96,256]{1,0:T(8,128)(2,1)S(1)}, u32[]{:S(2)}, u32[]{:S(2)}) collective-permute-start(bf16[96,256]{1,0:T(8,128)(2,1)S(1)} %get-tuple-element.44), channel_id=1, source_target_pairs={{0,3},{1,0},{2,1},{3,2},{4,7},{5,4},{6,5},{7,6},{8,11},{9,8},{10,9... | collective-permute-start | bytes 147464 | tf_op jit(solution)/shard_map/ppermute | solution.py:377
  153.6 5.6 %collective-permute-start.22 = (bf16[96,256]{1,0:T(8,128)(2,1)S(1)}, bf16[96,256]{1,0:T(8,128)(2,1)S(1)}, u32[]{:S(2)}, u32[]{:S(2)}) collective-permute-start(bf16[96,256]{1,0:T(8,128)(2,1)S(1)} %get-tuple-element.45), channel_id=1, source_target_pairs={{0,2},{1,3},{2,0},{3,1},{4,6},{5,7},{6,4},{7,5},{8,10},{9,11},{10,... | collective-permute-start | bytes 147464 | tf_op jit(solution)/shard_map/ppermute | solution.py:377

commit v2 on v1

--- a/solution.py
+++ b/solution.py
@@ -15,12 +15,12 @@
 SUM_LOW = 2.0**-80
 SUM_HIGH = 2.0**100
 VMEM = pl.BlockSpec(memory_space=pltpu.VMEM)
-QT = 768
 KT = 768
+TILES_C = (768, 384)
 
 
 def ring(n, k):
-    return [(i, (i + k) % n) for i in range(n)]
+    return [(i, i ^ k) for i in range(n)]
 
 
 def grid_move(step, first):
@@ -28,9 +28,9 @@
     for s in range(32):
         z, y, c = s // 8, (s // 2) % 4, s % 2
         if (c == 0) == first:
-            z = (z + step) % 4
+            z ^= step
         else:
-            y = (y + step) % 4
+            y ^= step
         pairs.append((s, z * 8 + y * 2 + c))
     return pairs
 
@@ -48,8 +48,8 @@
     row = lax.broadcasted_iota(jnp.int32, (64, 4 * n), 0)
     block = lax.div(lane, n)
     inside = lax.rem(lane, n)
-    shift = jnp.where(block == 0, 0, jnp.where(block == 1, 3, jnp.where(block == 2, 1, 2)))
-    place = sp * (4 * n) + ((tp + shift) & 3) * n + inside
+    shift = jnp.where(block == 0, 1, jnp.where(block == 1, 3, jnp.where(block == 2, 2, 0)))
+    place = sp * (4 * n) + (tp ^ shift) * n + inside
     freq = jnp.asarray(np.tile(ROPE_BASE ** (-np.arange(16) / 16.0), 4)[:, None], jnp.float32)
     angle = jnp.where(row < 32, place >> 6, place & 63).astype(jnp.float32) * freq
     return jnp.where((row & 16) == 0, jnp.cos(angle), jnp.sin(angle))
@@ -94,7 +94,7 @@
 def far_kernel(t3, t4, raw_own, raw_near, weight, gk, tab, kv_ref, raw_ref, raw):
     n = 2 * t3.shape[0]
     made = dot(jnp.concatenate([t3[...], t4[...]], axis=0), weight[...]).astype(jnp.bfloat16)
-    for at, part in ((0, raw_own[...]), (n, raw_near[...]), (3 * n, made)):
+    for at, part in ((0, raw_near[...]), (2 * n, made), (3 * n, raw_own[...])):
         raw[at : at + part.shape[0], :] = part[:, 256:]
         raw_ref[at : at + part.shape[0], :] = part[:, :256]
     kv_ref[...] = keys_values(raw[...], column(gk[...]), tab[...])
@@ -102,14 +102,18 @@
 
 def query_kernel(raw, gq, tab, qt_ref):
     count = raw.shape[0]
+    n = count // 4
     table = tab[...]
+    heads = []
     for h in range(4):
         if h % 2 == 0:
             both = raw[:, h * 64 : h * 64 + 128].astype(jnp.float32).T
         x = both[(h % 2) * 64 : (h % 2) * 64 + 64]
-        q = norm_turn(x, column(gq[h : h + 1, :]), table).astype(jnp.bfloat16)
-        qt_ref[0:64, h * count : (h + 1) * count] = q
-        qt_ref[64:128, h * count : (h + 1) * count] = jnp.zeros_like(q)
+        heads.append(norm_turn(x, column(gq[h : h + 1, :]), table))
+    for b in range(4):
+        q = jnp.concatenate([x[:, b * n : (b + 1) * n] for x in heads], axis=1).astype(jnp.bfloat16)
+        qt_ref[0:64, b * count : (b + 1) * count] = q
+        qt_ref[64:128, b * count : (b + 1) * count] = jnp.zeros_like(q)
 
 
 def join_kernel(*refs):
@@ -132,7 +136,7 @@
     )(*parts)
 
 
-def attend_kernel(*refs, n_kv, n_extra, first, last, scale, pieces):
+def attend_kernel(*refs, n_kv, n_extra, first, last, scale, pieces, span, tiles):
     refs = list(refs)
     qt_ref = refs.pop(0)
     kv_refs = [refs.pop(0) for _ in range(n_kv)]
@@ -140,14 +144,15 @@
     if not first:
         acc_in, l_in, m_in = [refs.pop(0) for _ in range(3)]
     if last:
-        att_refs = [refs.pop(0) for _ in range(4)]
-        lse_ref = refs.pop(0)
+        att_refs = [refs.pop(0) for _ in range((span[1] - span[0]) // 384)]
+        lse_refs = [refs.pop(0) for _ in att_refs]
         acc_ref, l_ref, m_ref = [refs.pop(0) for _ in range(3)]
     else:
         acc_ref, l_ref, m_ref = [refs.pop(0) for _ in range(3)]
     vt_ref, p_ref = refs
     c = scale * LOG2E
-    nq = qt_ref.shape[1]
+    low, nq = span[0], span[1] - span[0]
+    qt_ref = qt_ref.at[:, low : low + nq]
 
     def block(piece):
         parts = [kv_refs[j][r : r + size, :] for j, r, size in piece]
@@ -156,8 +161,10 @@
     for i, piece in enumerate(pieces):
         vt_ref[:, i * 384 : (i + 1) * 384] = block(piece).T[64:, :]
 
-    for qi in range(nq // QT):
-        cols = slice(qi * QT, (qi + 1) * QT)
+    ends = [sum(tiles[: i + 1]) for i in range(len(tiles))]
+    columns = [slice(e - t, e) for e, t in zip(ends, tiles)]
+    for cols in columns:
+        QT = cols.stop - cols.start
         if first:
             top = None
             for piece in pieces:
@@ -168,23 +175,21 @@
             acc_ref[:, cols] = jnp.zeros((64, QT), jnp.float32)
             l_ref[:, cols] = jnp.zeros((8, QT), jnp.float32)
         else:
-            m_ref[:, cols] = m_in[:, cols]
-            acc_ref[:, cols] = acc_in[:, cols]
-            l_ref[:, cols] = l_in[:, cols]
+            m_ref[:, cols] = m_in[:, low + cols.start : low + cols.stop]
+            acc_ref[:, cols] = acc_in[:, low + cols.start : low + cols.stop]
+            l_ref[:, cols] = l_in[:, low + cols.start : low + cols.stop]
 
     def weigh(step, slot, cols):
         for h in range(2):
             s = dot(block(pieces[2 * step + h]), qt_ref[:, cols])
             p = jnp.exp2(s * c - m_ref[:, cols])
-            l_ref[:, cols] += jnp.sum(p.reshape(48, 8, QT), axis=0)
-            p_ref[slot, h * 384 : (h + 1) * 384, :] = p.astype(jnp.bfloat16)
+            l_ref[:, cols] += jnp.sum(p.reshape(48, 8, p.shape[1]), axis=0)
+            p_ref[slot, h * 384 : (h + 1) * 384, : p.shape[1]] = p.astype(jnp.bfloat16)
 
     def gather_values(step, slot, cols):
-        acc_ref[:, cols] += dot(vt_ref[:, step * 768 : (step + 1) * 768], p_ref[slot])
-
-    steps = [
-        (i, slice(qi * QT, (qi + 1) * QT)) for qi in range(nq // QT) for i in range(len(pieces) // 2)
-    ]
+        acc_ref[:, cols] += dot(vt_ref[:, step * 768 : (step + 1) * 768], p_ref[slot, :, : cols.stop - cols.start])
+
+    steps = [(i, cols) for cols in columns for i in range(len(pieces) // 2)]
     before = None
     for t, (i, cols) in enumerate(steps):
         weigh(i, t % 2, cols)
@@ -230,26 +235,22 @@
         total = jnp.sum(l_ref[...], axis=0, keepdims=True)
         lse = (m_ref[...] + jnp.log2(total)) * (1.0 / LOG2E)
         out = acc_ref[...] / total
-        count = nq // 4
-        for h in range(0, 4, 2):
-            two = jnp.concatenate(
-                [out[:, h * count : (h + 1) * count], out[:, (h + 1) * count : (h + 2) * count]], axis=0
-            )
-            two = two.T.astype(jnp.bfloat16)
-            for i, ref in enumerate(att_refs):
-                ref[:, h * 64 : h * 64 + 128] = two[i * (count // 4) : (i + 1) * (count // 4)]
-        for h in range(4):
-            lse_ref[h : h + 1, :] = lse[:, h * count : (h + 1) * count]
-
-
-def attend(qt, kvs, pieces, extra, state, last, scale):
-    nq = qt.shape[1]
+        n = 96
+        for b, (att_ref, lse_ref) in enumerate(zip(att_refs, lse_refs)):
+            heads = [slice(b * 384 + h * n, b * 384 + (h + 1) * n) for h in range(4)]
+            att_ref[...] = jnp.concatenate([out[:, h] for h in heads], axis=0).T.astype(jnp.bfloat16)
+            lse_ref[...] = jnp.concatenate([lse[:, h] for h in heads], axis=0)
+
+
+def attend(qt, kvs, pieces, extra, state, last, scale, span, tiles):
+    nq = span[1] - span[0]
     keys = 384 * len(pieces)
     f32 = jnp.float32
     parts = (jax.ShapeDtypeStruct((64, nq), f32), jax.ShapeDtypeStruct((8, nq), f32), jax.ShapeDtypeStruct((1, nq), f32))
-    scratch = [pltpu.VMEM((64, keys), jnp.bfloat16), pltpu.VMEM((2, KT, QT), jnp.bfloat16)]
+    scratch = [pltpu.VMEM((64, keys), jnp.bfloat16), pltpu.VMEM((2, KT, max(tiles)), jnp.bfloat16)]
     if last:
-        outs = (jax.ShapeDtypeStruct((nq // 16, 256), jnp.bfloat16),) * 4 + (jax.ShapeDtypeStruct((4, nq // 4), f32),)
+        blocks = nq // 384
+        outs = (jax.ShapeDtypeStruct((96, 256), jnp.bfloat16),) * blocks + (jax.ShapeDtypeStruct((4, 96), f32),) * blocks
         scratch = [pltpu.VMEM(p.shape, f32) for p in parts] + scratch
     else:
         outs = parts
@@ -258,6 +259,8 @@
         functools.partial(
             attend_kernel, n_kv=len(kvs), n_extra=len(extra), first=state is None, last=last, scale=scale,
             pieces=pieces,
+            span=span,
+            tiles=tiles,
         ),
         out_shape=outs,
         in_specs=[VMEM] * len(args),
@@ -270,19 +273,18 @@
     )(*args)
 
 
-def early_kernel(place, lse, a0, w0, w1, w2, w3, x1, x2, x3, part_ref, rows_ref, lse_ref):
+def early_kernel(place, s0, s1, s2, s3, a0, w0, w1, w2, w3, x1, x2, x3, part_ref, rows_ref, lse_ref):
     half = w1.shape[0]
     part_ref[...] = dot(a0[...], w0[...])
     for i, (w, x) in enumerate(((w1, x1), (w2, x2), (w3, x3))):
         rows_ref[pl.ds(pl.multiple_of((2 * i + place[0]) * half, half), half), :] = w[...]
         rows_ref[pl.ds(pl.multiple_of((2 * i + 1 - place[0]) * half, half), half), :] = x[...]
-    n = lse.shape[1] // 4
-    cyc = [lse[:, i * n : (i + 1) * n] for i in (0, 2, 3, 1)]
+    sums = [s3[...], s0[...], s2[...], s1[...]]
     for t in range(4):
 
         @pl.when(place[1] == t)
         def _():
-            lse_ref[...] = jnp.concatenate([cyc[(a - t) % 4] for a in range(4)], axis=1)
+            lse_ref[...] = jnp.concatenate([sums[a ^ t] for a in range(4)], axis=1)
 
 
 def mix_kernel(part, a1, a2, a3, rows, out_ref):
@@ -303,8 +305,8 @@
 
     from_left = lax.ppermute(tokens, "tp", ring(4, 1))
     from_right = lax.ppermute(tokens, "tp", ring(4, 3))
-    far_a = lax.ppermute(from_left[: n // 2], "tp", ring(4, 1))
-    far_b = lax.ppermute(from_right[n // 2 :], "tp", ring(4, 3))
+    far_a = lax.ppermute(from_right[: n // 2], "tp", ring(4, 1))
+    far_b = lax.ppermute(from_left[n // 2 :], "tp", ring(4, 3))
     table = angle_rows(sp, tp, n)
     half = out_weight.shape[0] // 2
     raw_own, weight, mine = pl.pallas_call(
@@ -365,15 +367,19 @@
     def quarters(j):
         return [((j, 384 * i, 384),) for i in range(4)]
 
-    state = attend(qt, [load, load_twin], quarters(0) + quarters(1), [], None, False, scale)
-    state = attend(qt, plane, quarters(0) + quarters(1) + quarters(2), [], state, False, scale)
+    full, twice = (0, 16 * n), (768, 768)
+    twelve = quarters(0) + quarters(1) + quarters(2)
+    state = attend(qt, [load, load_twin], quarters(0) + quarters(1), [], None, False, scale, full, twice)
+    state = attend(qt, plane, twelve, [], state, False, scale, full, twice)
     rows_in = lax.optimization_barrier((*rows_in, state[2]))[:3]
     rows_other = [lax.ppermute(w, "sp", core_swap()) for w in rows_in]
-    *att, lse = attend(
-        qt, plane_twin, quarters(0) + quarters(1) + quarters(2), [load, load_twin, *plane], state, True, scale
-    )
+    others = [load, load_twin, *plane]
+    *made, = attend(qt, plane_twin, twelve, others, state, True, scale, (0, 12 * n), TILES_C)
+    att, sums = made[:3], made[3:]
+    own, own_sums = attend(qt, plane_twin, twelve, others, state, True, scale, (12 * n, 16 * n), (384,))
+    sums = [*sums, own_sums]
     back = []
-    for i, k in ((2, 1), (1, 3), (3, 2)):
+    for i, k in ((0, 1), (1, 3), (2, 2)):
         back.append(lax.ppermute(att[i], "tp", ring(4, k)))
     wide = out_weight.shape[1]
     part, rows, log_sums = pl.pallas_call(
@@ -383,11 +389,11 @@
             jax.ShapeDtypeStruct((6 * half, wide), bf16),
             jax.ShapeDtypeStruct((4, 4 * n), jnp.float32),
         ),
-        in_specs=[pl.BlockSpec(memory_space=pltpu.SMEM)] + [VMEM] * 9,
+        in_specs=[pl.BlockSpec(memory_space=pltpu.SMEM)] + [VMEM] * 12,
         out_specs=(VMEM,) * 3,
         compiler_params=small,
         cost_estimate=pl.CostEstimate(flops=2 * n * 256 * 2048, bytes_accessed=2**22, transcendentals=0),
-    )(place, lse, att[0], out_weight, *rows_in, *rows_other)
+    )(place, *sums, own, out_weight, *rows_in, *rows_other)
     mixed = pl.pallas_call(
         mix_kernel,
         out_shape=jax.ShapeDtypeStruct((n, wide), bf16),

time: 161 us -> 218 us (1.35)
  Pallas kernels: 105 us -> 162 us
  starting transfers between devices: 27.4 us -> 22.6 us
  waiting for transfers between devices: 21.5 us -> 25.8 us
    pallas_call x3 -> x4, Pallas kernels: 99.4 us -> 156 us  [attend(): pl.pallas_call(functools.partial(attend_kernel, n_kv=len(kvs), n_extra=le...]
    ppermute x3, waiting for transfers between devices: 3.22 us -> 0.01 us  [body(): back.append(lax.ppermute(att[i], 'tp', ring(4, k)))]
    ppermute x1, waiting for transfers between devices: 0.01 us -> 2.58 us  [body(): from_right = lax.ppermute(tokens, 'tp', ring(4, 3))]
  transfers between devices with their start and end apart: 23 -> 23, of which waited for: 10 -> 11; matrix products, arithmetic and copies ran while one was open for 0% -> 0% of each run, Pallas kernels for 64% -> 74%
where the time goes in v2:
time: 218 us; the launch traced here: 217 us
  Pallas kernels  162 us (74%)
  waiting for transfers between devices  25.8 us (12%)
  starting transfers between devices  22.6 us (10%)
  local copies, waits for them, and re-layouts  5.39 us (2%)
    pallas_call x4, Pallas kernels, attend(): pl.pallas_call(functools.partial(attend_kernel, n_kv=len(kvs), n_extra=le...  156 us
    ppermute x3, waiting for transfers between devices, body(): plane.append(lax.ppermute(load, 'sp', grid_move(k, False)))  6.65 us
    unnamed x18, local copies, waits for them, and re-layouts  5.37 us
    ppermute x3, starting transfers between devices, body(): line.append(lax.ppermute(kv, 'sp', grid_move(k, True)))  4.97 us
    ppermute x3, waiting for transfers between devices, body(): line.append(lax.ppermute(kv, 'sp', grid_move(k, True)))  4.81 us
    ppermute x3, waiting for transfers between devices, body(): rows_in.append(lax.ppermute(mine, 'tp', ring(4, k)))  4.7 us
  transfers between devices with their start and end apart: 23, of which 11 were waited for; matrix products, arithmetic and copies ran while one was open for 0% of the time, Pallas kernels for 74%

profile of v2, /device:TPU:0, one launch (start us, length us, event | category | flops | bytes accessed | tf_op | source)
XLA Modules:
  0.0 217.3 jit_solution(18163335905095865169)
XLA Ops:
  0.6 0.0 copy-start.8
  0.6 2.9 %collective-permute-start = (bf16[96,2048]{1,0:T(8,128)(2,1)}, bf16[96,2048]{1,0:T(8,128)(2,1)S(1)}, u32[]{:S(2)}, u32[]{:S(2)}) collective-permute-start(bf16[96,2048]{1,0:T(8,128)(2,1)} %t0.1), channel_id=1, source_target_pairs={{0,3},{1,2},{2,1},{3,0},{4,7},{5,6},{6,5},{7,4},{8,11},{9,10},{10,... | collective-permute-start | bytes 1179656 | tf_op jit(solution)/shard_map/ppermute | solution.py:307
  3.6 0.2 collective-permute-start.2
  3.8 0.1 pad_add_fusion.place
  3.9 1.2 copy-done
  5.1 1.2 copy-done.2
  6.3 1.0 copy-done.3
  7.3 0.9 copy-done.4
  8.3 0.9 copy-done.5
  9.2 1.1 shard_map.95
  10.3 2.6 %collective-permute-done.t2 = bf16[96,2048]{1,0:T(8,128)(2,1)S(1)} collective-permute-done((bf16[96,2048]{1,0:T(8,128)(2,1)}, bf16[96,2048]{1,0:T(8,128)(2,1)S(1)}, u32[]{:S(2)}, u32[]{:S(2)}) %collective-permute-start) | collective-permute-done | bytes 393248 | tf_op jit(solution)/shard_map/ppermute | solution.py:307
  12.9 0.0 copy-start.6
  12.9 0.6 collective-permute-start.1
  13.5 0.9 collective-permute-done.2.t1
  14.4 1.7 collective-permute-start.3
  16.1 0.4 sine_select_fusion.tab
  16.5 0.7 shard_map.96.raw_near
  17.2 1.5 collective-permute-done.1.t3
  18.7 2.6 %collective-permute-done.3.t4 = bf16[48,2048]{1,0:T(8,128)(2,1)S(1)} collective-permute-done((bf16[48,2048]{1,0:T(8,128)(2,1)S(1)}, bf16[48,2048]{1,0:T(8,128)(2,1)S(1)}, u32[]{:S(2)}, u32[]{:S(2)}) %collective-permute-start.3) | collective-permute-done | bytes 196640 | tf_op jit(solution)/shard_map/ppermute | solution.py:309
  21.4 0.6 shard_map.97
  22.0 4.0 %collective-permute-start.6 = (bf16[384,128]{1,0:T(8,128)(2,1)S(1)}, bf16[384,128]{1,0:T(8,128)(2,1)S(1)}, u32[]{:S(2)}, u32[]{:S(2)}) collective-permute-start(bf16[384,128]{1,0:T(8,128)(2,1)S(1)} %get-tuple-element.31.refs_0_), channel_id=1, source_target_pairs={{0,64},{4,20},{8,72},{12,28},{16,80},{20,4},{24,88},{28,12},{32,96... | collective-permute-start | bytes 294920 | tf_op jit(solution)/shard_map/ppermute | solution.py:343
  25.9 0.7 collective-permute-start.5
  26.6 0.3 collective-permute-start.4
  26.9 1.6 collective-permute-done.6.refs_3_
  28.5 3.2 %collective-permute-done.5.refs_2_ = bf16[384,128]{1,0:T(8,128)(2,1)S(1)} collective-permute-done((bf16[384,128]{1,0:T(8,128)(2,1)S(1)}, bf16[384,128]{1,0:T(8,128)(2,1)S(1)}, u32[]{:S(2)}, u32[]{:S(2)}) %collective-permute-start.5) | collective-permute-done | bytes 98336 | tf_op jit(solution)/shard_map/ppermute | solution.py:343
  31.8 0.0 collective-permute-done.4.refs_1_
  31.8 0.1 collective-permute-start.13
  31.9 3.3 %collective-permute-start.11 = (bf16[1536,128]{1,0:T(8,128)(2,1)S(1)}, bf16[1536,128]{1,0:T(8,128)(2,1)S(1)}, u32[]{:S(2)}, u32[]{:S(2)}) collective-permute-start(bf16[1536,128]{1,0:T(8,128)(2,1)S(1)} %shard_map.99.refs_1_.refs_4_), channel_id=1, source_target_pairs={{0,16},{4,68},{8,24},{12,76},{16,0},{20,84},{24,8},{28,92},{32,48}... | collective-permute-start | bytes 1179656 | tf_op jit(solution)/shard_map/ppermute | solution.py:356
  35.2 1.1 collective-permute-start.9
  36.2 0.0 collective-permute-start.7
  36.2 1.9 collective-permute-start.16
  38.1 0.0 collective-permute-done.13.refs_2_.refs_5_
  38.1 0.7 collective-permute-start.15
  38.8 2.5 %collective-permute-done.11.refs_3_.refs_8_ = bf16[1536,128]{1,0:T(8,128)(2,1)S(1)} collective-permute-done((bf16[1536,128]{1,0:T(8,128)(2,1)S(1)}, bf16[1536,128]{1,0:T(8,128)(2,1)S(1)}, u32[]{:S(2)}, u32[]{:S(2)}) %collective-permute-start.11) | collective-permute-done | bytes 393248 | tf_op jit(solution)/shard_map/ppermute | solution.py:356
  41.3 0.0 collective-permute-start.14
  41.3 4.1 %collective-permute-done.9.refs_2_.refs_7_ = bf16[1536,128]{1,0:T(8,128)(2,1)S(1)} collective-permute-done((bf16[1536,128]{1,0:T(8,128)(2,1)S(1)}, bf16[1536,128]{1,0:T(8,128)(2,1)S(1)}, u32[]{:S(2)}, u32[]{:S(2)}) %collective-permute-start.9) | collective-permute-done | bytes 393248 | tf_op jit(solution)/shard_map/ppermute | solution.py:356
  45.5 0.0 collective-permute-start.12
  45.5 0.4 shard_map.98.refs_0_
  45.8 4.7 %shard_map.100 = (f32[64,1536]{1,0:T(8,128)S(1)}, f32[8,1536]{1,0:T(8,128)S(1)}, f32[1,1536]{1,0:T(1,128)S(1)}) custom-call(bf16[128,1536]{1,0:T(8,128)(2,1)S(1)} %shard_map.98.refs_0_, bf16[1536,128]{1,0:T(8,128)(2,1)S(1)} %shard_map.99.refs_1_.refs_4_, bf16[1536,128]{1,0:T(8,128)(2,1)S(1)} %collective-permute-done.13.refs_2_.refs_5_), custom_call_target="tpu_custom_call" | custom-call | flops 1207959552 | bytes 1572864 | tf_op jit(solution)/shard_map/pallas_call | solution.py:258
  50.5 0.0 collective-permute-done.7.refs_1_.refs_6_
  50.5 6.4 %shard_map.101 = (f32[64,1536]{1,0:T(8,128)S(1)}, f32[8,1536]{1,0:T(8,128)S(1)}, f32[1,1536]{1,0:T(1,128)S(1)}) custom-call(bf16[128,1536]{1,0:T(8,128)(2,1)S(1)} %shard_map.98.refs_0_, bf16[1536,128]{1,0:T(8,128)(2,1)S(1)} %collective-permute-done.7.refs_1_.refs_6_, bf16[1536,128]{1,0:T(8,128)(2,1)S(1)} %collective-permute-done.9.refs_2_.refs_7_, ...), custom_call_target="tpu_custom_call" | custom-call | flops 1811939328 | bytes 1966080 | tf_op jit(solution)/shard_map/pallas_call | solution.py:258
  56.9 0.0 collective-permute-done.16.w3
  56.9 4.7 %collective-permute-done.15.w2 = bf16[128,2048]{1,0:T(8,128)(2,1)S(1)} collective-permute-done((bf16[128,2048]{1,0:T(8,128)(2,1)S(1)}, bf16[128,2048]{1,0:T(8,128)(2,1)S(1)}, u32[]{:S(2)}, u32[]{:S(2)}) %collective-permute-start.15) | collective-permute-done | bytes 524320 | tf_op jit(solution)/shard_map/ppermute | solution.py:365
  61.6 0.0 collective-permute-done.14.w1
  61.6 0.0 collective-permute-start.17
  61.6 0.5 collective-permute-start.10
  62.1 0.0 collective-permute-start.8
  62.1 0.5 collective-permute-start.18
  62.6 0.0 collective-permute-done.12.refs_3_
  62.6 0.0 collective-permute-start.19
  62.6 1.4 collective-permute-done.10.refs_2_
  64.1 0.6 collective-permute-done.8.refs_1_
  64.6 81.9 %shard_map.102 = (bf16[96,256]{1,0:T(8,128)(2,1)S(1)}, bf16[96,256]{1,0:T(8,128)(2,1)S(1)}, bf16[96,256]{1,0:T(8,128)(2,1)S(1)}, f32[4,96]{1,0:T(4,128)S(1)}, f32[4,96]{1,0:T(4,128)S(1)}, /*index=5*/f32[4,96]{1,0:T(4,128)S(1)}) custom-call(bf16[128,1536]{1,0:T(8,128)(2,1)S(1)} %shard_map.98.refs_0_, bf16[1536,128]{1,0:T(8,128)(2,1)S(1)} %collective-permute-done.8.refs_1_, ...), custom_call_target="tpu_custom_call" | custom-call | flops 1358954496 | bytes 1769472 | tf_op jit(solution)/shard_map/pallas_call | solution.py:258
  146.6 0.0 copy-start.1
  146.6 0.5 collective-permute-start.20
  147.0 1.9 collective-permute-start.21
  149.0 0.0 collective-permute-done.17.x1
  149.0 1.8 collective-permute-start.22
  150.7 63.5 %shard_map.103 = (bf16[96,256]{1,0:T(8,128)(2,1)S(1)}, f32[4,96]{1,0:T(4,128)S(1)}) custom-call(bf16[128,1536]{1,0:T(8,128)(2,1)S(1)} %shard_map.98.refs_0_, bf16[1536,128]{1,0:T(8,128)(2,1)S(1)} %collective-permute-done.8.refs_1_, bf16[1536,128]{1,0:T(8,128)(2,1)S(1)} %collective-permute-done.10.refs_2_, ...), custom_call_target="tpu_custom_call" | custom-call | flops 452984832 | bytes 1376256 | tf_op jit(solution)/shard_map/pallas_call | solution.py:258
  214.2 1.6 shard_map.104
  215.9 0.0 collective-permute-done.20.a1
  215.9 0.0 collective-permute-done.21.a2
  215.9 0.0 collective-permute-done.22.a3
  215.9 1.4 shard_map.105
  (18 shorter events, 0.1 us)
Async XLA Ops:
  0.6 15.5 %copy-start.8 = (f32[64]{0:T(128)S(1)}, f32[64]{0:T(128)}, u32[]{:S(2)}) copy-start(f32[64]{0:T(128)} %constant.37) | copy-start | bytes 772
  0.6 12.3 %collective-permute-start = (bf16[96,2048]{1,0:T(8,128)(2,1)}, bf16[96,2048]{1,0:T(8,128)(2,1)S(1)}, u32[]{:S(2)}, u32[]{:S(2)}) collective-permute-start(bf16[96,2048]{1,0:T(8,128)(2,1)} %t0.1), channel_id=1, source_target_pairs={{0,3},{1,2},{2,1},{3,0},{4,7},{5,6},{6,5},{7,4},{8,11},{9,10},{10,... | collective-permute-start | bytes 1179656 | tf_op jit(solution)/shard_map/ppermute | solution.py:307
  3.6 10.8 %collective-permute-start.2 = (bf16[96,2048]{1,0:T(8,128)(2,1)}, bf16[96,2048]{1,0:T(8,128)(2,1)S(1)}, u32[]{:S(2)}, u32[]{:S(2)}) collective-permute-start(bf16[96,2048]{1,0:T(8,128)(2,1)} %t0.1), channel_id=1, source_target_pairs={{0,1},{1,0},{2,3},{3,2},{4,5},{5,4},{6,7},{7,6},{8,9},{9,8},{10,11... | collective-permute-start | bytes 1179656 | tf_op jit(solution)/shard_map/ppermute | solution.py:306
  3.9 1.2 copy-start
  5.1 1.2 copy-start.2
  6.3 1.0 copy-start.3
  7.3 0.9 copy-start.4
  8.3 0.9 copy-start.5
  9.2 12.1 %copy-start.7 = (bf16[1,64]{1,0:T(2,128)(2,1)S(1)}, bf16[1,64]{1,0:T(2,128)(2,1)}, u32[]{:S(2)}) copy-start(bf16[1,64]{1,0:T(2,128)(2,1)} %gk.1) | copy-start | bytes 388
  12.9 32.5 %copy-start.6 = (bf16[4,64]{1,0:T(4,128)(2,1)S(1)}, bf16[4,64]{1,0:T(4,128)(2,1)}, u32[]{:S(2)}) copy-start(bf16[4,64]{1,0:T(4,128)(2,1)} %gq.1) | copy-start | bytes 1540
  12.9 5.8 %collective-permute-start.1 = (bf16[48,2048]{1,0:T(8,128)(2,1)S(1)}, bf16[48,2048]{1,0:T(8,128)(2,1)S(1)}, u32[]{:S(2)}, u32[]{:S(2)}) collective-permute-start(bf16[48,2048]{1,0:T(8,128)(2,1)S(1)} %slice.8), channel_id=1, source_target_pairs={{0,1},{1,0},{2,3},{3,2},{4,5},{5,4},{6,7},{7,6},{8,9},{9,8},{10,11... | collective-permute-start | bytes 589832 | tf_op jit(solution)/shard_map/ppermute | solution.py:308
  14.4 7.0 %collective-permute-start.3 = (bf16[48,2048]{1,0:T(8,128)(2,1)S(1)}, bf16[48,2048]{1,0:T(8,128)(2,1)S(1)}, u32[]{:S(2)}, u32[]{:S(2)}) collective-permute-start(bf16[48,2048]{1,0:T(8,128)(2,1)S(1)} %slice.9), channel_id=1, source_target_pairs={{0,3},{1,2},{2,1},{3,0},{4,7},{5,6},{6,5},{7,4},{8,11},{9,10},{10,... | collective-permute-start | bytes 589832 | tf_op jit(solution)/shard_map/ppermute | solution.py:309
  22.0 6.6 %collective-permute-start.6 = (bf16[384,128]{1,0:T(8,128)(2,1)S(1)}, bf16[384,128]{1,0:T(8,128)(2,1)S(1)}, u32[]{:S(2)}, u32[]{:S(2)}) collective-permute-start(bf16[384,128]{1,0:T(8,128)(2,1)S(1)} %get-tuple-element.31.refs_0_), channel_id=1, source_target_pairs={{0,64},{4,20},{8,72},{12,28},{16,80},{20,4},{24,88},{28,12},{32,96... | collective-permute-start | bytes 294920 | tf_op jit(solution)/shard_map/ppermute | solution.py:343
  25.9 5.8 %collective-permute-start.5 = (bf16[384,128]{1,0:T(8,128)(2,1)S(1)}, bf16[384,128]{1,0:T(8,128)(2,1)S(1)}, u32[]{:S(2)}, u32[]{:S(2)}) collective-permute-start(bf16[384,128]{1,0:T(8,128)(2,1)S(1)} %get-tuple-element.31.refs_0_), channel_id=1, source_target_pairs={{0,96},{4,28},{8,104},{12,20},{16,112},{20,12},{24,120},{28,4},{32... | collective-permute-start | bytes 294920 | tf_op jit(solution)/shard_map/ppermute | solution.py:343
  26.6 5.1 %collective-permute-start.4 = (bf16[384,128]{1,0:T(8,128)(2,1)S(1)}, bf16[384,128]{1,0:T(8,128)(2,1)S(1)}, u32[]{:S(2)}, u32[]{:S(2)}) collective-permute-start(bf16[384,128]{1,0:T(8,128)(2,1)S(1)} %get-tuple-element.31.refs_0_), channel_id=1, source_target_pairs={{0,32},{4,12},{8,40},{12,4},{16,48},{20,28},{24,56},{28,20},{32,0}... | collective-permute-start | bytes 294920 | tf_op jit(solution)/shard_map/ppermute | solution.py:343
  31.8 6.3 %collective-permute-start.13 = (bf16[1536,128]{1,0:T(8,128)(2,1)S(1)}, bf16[1536,128]{1,0:T(8,128)(2,1)S(1)}, u32[]{:S(2)}, u32[]{:S(2)}) collective-permute-start(bf16[1536,128]{1,0:T(8,128)(2,1)S(1)} %shard_map.99.refs_1_.refs_4_), channel_id=1, source_target_pairs={{0,4},{4,0},{8,12},{12,8},{16,20},{20,16},{24,28},{28,24},{32,36},... | collective-permute-start | bytes 1179656 | tf_op jit(solution)/shard_map/ppermute | solution.py:357
  31.9 9.5 %collective-permute-start.11 = (bf16[1536,128]{1,0:T(8,128)(2,1)S(1)}, bf16[1536,128]{1,0:T(8,128)(2,1)S(1)}, u32[]{:S(2)}, u32[]{:S(2)}) collective-permute-start(bf16[1536,128]{1,0:T(8,128)(2,1)S(1)} %shard_map.99.refs_1_.refs_4_), channel_id=1, source_target_pairs={{0,16},{4,68},{8,24},{12,76},{16,0},{20,84},{24,8},{28,92},{32,48}... | collective-permute-start | bytes 1179656 | tf_op jit(solution)/shard_map/ppermute | solution.py:356
  35.2 10.3 %collective-permute-start.9 = (bf16[1536,128]{1,0:T(8,128)(2,1)S(1)}, bf16[1536,128]{1,0:T(8,128)(2,1)S(1)}, u32[]{:S(2)}, u32[]{:S(2)}) collective-permute-start(bf16[1536,128]{1,0:T(8,128)(2,1)S(1)} %shard_map.99.refs_1_.refs_4_), channel_id=1, source_target_pairs={{0,24},{4,100},{8,16},{12,108},{16,8},{20,116},{24,0},{28,124},{32... | collective-permute-start | bytes 1179656 | tf_op jit(solution)/shard_map/ppermute | solution.py:356
  36.2 14.3 %collective-permute-start.7 = (bf16[1536,128]{1,0:T(8,128)(2,1)S(1)}, bf16[1536,128]{1,0:T(8,128)(2,1)S(1)}, u32[]{:S(2)}, u32[]{:S(2)}) collective-permute-start(bf16[1536,128]{1,0:T(8,128)(2,1)S(1)} %shard_map.99.refs_1_.refs_4_), channel_id=1, source_target_pairs={{0,8},{4,36},{8,0},{12,44},{16,24},{20,52},{24,16},{28,60},{32,40}... | collective-permute-start | bytes 1179656 | tf_op jit(solution)/shard_map/ppermute | solution.py:356
  36.2 20.7 %collective-permute-start.16 = (bf16[128,2048]{1,0:T(8,128)(2,1)S(1)}, bf16[128,2048]{1,0:T(8,128)(2,1)S(1)}, u32[]{:S(2)}, u32[]{:S(2)}) collective-permute-start(bf16[128,2048]{1,0:T(8,128)(2,1)S(1)} %get-tuple-element.44), channel_id=1, source_target_pairs={{0,2},{1,3},{2,0},{3,1},{4,6},{5,7},{6,4},{7,5},{8,10},{9,11},{10,... | collective-permute-start | bytes 1572872 | tf_op jit(solution)/shard_map/ppermute | solution.py:365
  38.1 23.5 %collective-permute-start.15 = (bf16[128,2048]{1,0:T(8,128)(2,1)S(1)}, bf16[128,2048]{1,0:T(8,128)(2,1)S(1)}, u32[]{:S(2)}, u32[]{:S(2)}) collective-permute-start(bf16[128,2048]{1,0:T(8,128)(2,1)S(1)} %get-tuple-element.44), channel_id=1, source_target_pairs={{0,3},{1,2},{2,1},{3,0},{4,7},{5,6},{6,5},{7,4},{8,11},{9,10},{10,... | collective-permute-start | bytes 1572872 | tf_op jit(solution)/shard_map/ppermute | solution.py:365
  41.3 20.3 %collective-permute-start.14 = (bf16[128,2048]{1,0:T(8,128)(2,1)S(1)}, bf16[128,2048]{1,0:T(8,128)(2,1)S(1)}, u32[]{:S(2)}, u32[]{:S(2)}) collective-permute-start(bf16[128,2048]{1,0:T(8,128)(2,1)S(1)} %get-tuple-element.44), channel_id=1, source_target_pairs={{0,1},{1,0},{2,3},{3,2},{4,5},{5,4},{6,7},{7,6},{8,9},{9,8},{10,11... | collective-permute-start | bytes 1572872 | tf_op jit(solution)/shard_map/ppermute | solution.py:365
  45.5 17.2 %collective-permute-start.12 = (bf16[1536,128]{1,0:T(8,128)(2,1)S(1)}, bf16[1536,128]{1,0:T(8,128)(2,1)S(1)}, u32[]{:S(2)}, u32[]{:S(2)}) collective-permute-start(bf16[1536,128]{1,0:T(8,128)(2,1)S(1)} %collective-permute-done.11.refs_3_.refs_8_), channel_id=1, source_target_pairs={{0,4},{4,0},{8,12},{12,8},{16,20},{20,16},{24,28},{28,24},{32,36},... | collective-permute-start | bytes 1179656 | tf_op jit(solution)/shard_map/ppermute | solution.py:360
  61.6 87.4 %collective-permute-start.17 = (bf16[128,2048]{1,0:T(8,128)(2,1)S(1)}, bf16[128,2048]{1,0:T(8,128)(2,1)S(1)}, u32[]{:S(2)}, u32[]{:S(2)}) collective-permute-start(bf16[128,2048]{1,0:T(8,128)(2,1)S(1)} %collective-permute-done.14.w1), channel_id=1, source_target_pairs={{0,4},{4,0},{8,12},{12,8},{16,20},{20,16},{24,28},{28,24},{32,36},... | collective-permute-start | bytes 1572872 | tf_op jit(solution)/shard_map/ppermute | solution.py:375
  61.6 2.5 %collective-permute-start.10 = (bf16[1536,128]{1,0:T(8,128)(2,1)S(1)}, bf16[1536,128]{1,0:T(8,128)(2,1)S(1)}, u32[]{:S(2)}, u32[]{:S(2)}) collective-permute-start(bf16[1536,128]{1,0:T(8,128)(2,1)S(1)} %collective-permute-done.9.refs_2_.refs_7_), channel_id=1, source_target_pairs={{0,4},{4,0},{8,12},{12,8},{16,20},{20,16},{24,28},{28,24},{32,36},... | collective-permute-start | bytes 1179656 | tf_op jit(solution)/shard_map/ppermute | solution.py:360
  62.1 2.5 %collective-permute-start.8 = (bf16[1536,128]{1,0:T(8,128)(2,1)S(1)}, bf16[1536,128]{1,0:T(8,128)(2,1)S(1)}, u32[]{:S(2)}, u32[]{:S(2)}) collective-permute-start(bf16[1536,128]{1,0:T(8,128)(2,1)S(1)} %collective-permute-done.7.refs_1_.refs_6_), channel_id=1, source_target_pairs={{0,4},{4,0},{8,12},{12,8},{16,20},{20,16},{24,28},{28,24},{32,36},... | collective-permute-start | bytes 1179656 | tf_op jit(solution)/shard_map/ppermute | solution.py:360
  62.1 152.1 %collective-permute-start.18 = (bf16[128,2048]{1,0:T(8,128)(2,1)S(1)}, bf16[128,2048]{1,0:T(8,128)(2,1)S(1)}, u32[]{:S(2)}, u32[]{:S(2)}) collective-permute-start(bf16[128,2048]{1,0:T(8,128)(2,1)S(1)} %collective-permute-done.15.w2), channel_id=1, source_target_pairs={{0,4},{4,0},{8,12},{12,8},{16,20},{20,16},{24,28},{28,24},{32,36},... | collective-permute-start | bytes 1572872 | tf_op jit(solution)/shard_map/ppermute | solution.py:375
  62.6 151.6 %collective-permute-start.19 = (bf16[128,2048]{1,0:T(8,128)(2,1)S(1)}, bf16[128,2048]{1,0:T(8,128)(2,1)S(1)}, u32[]{:S(2)}, u32[]{:S(2)}) collective-permute-start(bf16[128,2048]{1,0:T(8,128)(2,1)S(1)} %collective-permute-done.16.w3), channel_id=1, source_target_pairs={{0,4},{4,0},{8,12},{12,8},{16,20},{20,16},{24,28},{28,24},{32,36},... | collective-permute-start | bytes 1572872 | tf_op jit(solution)/shard_map/ppermute | solution.py:375
  146.6 67.7 %copy-start.1 = (bf16[256,2048]{1,0:T(8,128)(2,1)S(1)}, bf16[256,2048]{1,0:T(8,128)(2,1)}, u32[]{:S(2)}) copy-start(bf16[256,2048]{1,0:T(8,128)(2,1)} %w0.1) | copy-start | bytes 3145732
  146.6 69.3 %collective-permute-start.20 = (bf16[96,256]{1,0:T(8,128)(2,1)S(1)}, bf16[96,256]{1,0:T(8,128)(2,1)S(1)}, u32[]{:S(2)}, u32[]{:S(2)}) collective-permute-start(bf16[96,256]{1,0:T(8,128)(2,1)S(1)} %get-tuple-element.49), channel_id=1, source_target_pairs={{0,1},{1,0},{2,3},{3,2},{4,5},{5,4},{6,7},{7,6},{8,9},{9,8},{10,11... | collective-permute-start | bytes 147464 | tf_op jit(solution)/shard_map/ppermute | solution.py:383
  147.0 68.9 %collective-permute-start.21 = (bf16[96,256]{1,0:T(8,128)(2,1)S(1)}, bf16[96,256]{1,0:T(8,128)(2,1)S(1)}, u32[]{:S(2)}, u32[]{:S(2)}) collective-permute-start(bf16[96,256]{1,0:T(8,128)(2,1)S(1)} %get-tuple-element.50), channel_id=1, source_target_pairs={{0,3},{1,2},{2,1},{3,0},{4,7},{5,6},{6,5},{7,4},{8,11},{9,10},{10,... | collective-permute-start | bytes 147464 | tf_op jit(solution)/shard_map/ppermute | solution.py:383
  149.0 66.9 %collective-permute-start.22 = (bf16[96,256]{1,0:T(8,128)(2,1)S(1)}, bf16[96,256]{1,0:T(8,128)(2,1)S(1)}, u32[]{:S(2)}, u32[]{:S(2)}) collective-permute-start(bf16[96,256]{1,0:T(8,128)(2,1)S(1)} %get-tuple-element.51), channel_id=1, source_target_pairs={{0,2},{1,3},{2,0},{3,1},{4,6},{5,7},{6,4},{7,5},{8,10},{9,11},{10,... | collective-permute-start | bytes 147464 | tf_op jit(solution)/shard_map/ppermute | solution.py:383

commit v3 on v2

--- a/solution.py
+++ b/solution.py
@@ -92,7 +92,7 @@
 
 
 def far_kernel(t3, t4, raw_own, raw_near, weight, gk, tab, kv_ref, raw_ref, raw):
-    n = 2 * t3.shape[0]
+    n = t3.shape[0] + t4.shape[0]
     made = dot(jnp.concatenate([t3[...], t4[...]], axis=0), weight[...]).astype(jnp.bfloat16)
     for at, part in ((0, raw_near[...]), (2 * n, made), (3 * n, raw_own[...])):
         raw[at : at + part.shape[0], :] = part[:, 256:]
@@ -305,8 +305,8 @@
 
     from_left = lax.ppermute(tokens, "tp", ring(4, 1))
     from_right = lax.ppermute(tokens, "tp", ring(4, 3))
-    far_a = lax.ppermute(from_right[: n // 2], "tp", ring(4, 1))
-    far_b = lax.ppermute(from_left[n // 2 :], "tp", ring(4, 3))
+    far_a = lax.ppermute(from_right[: 2 * n // 3], "tp", ring(4, 1))
+    far_b = lax.ppermute(from_left[2 * n // 3 :], "tp", ring(4, 3))
     table = angle_rows(sp, tp, n)
     half = out_weight.shape[0] // 2
     raw_own, weight, mine = pl.pallas_call(

time: 218 us -> 221 us (1.014)
  starting transfers between devices: 22.6 us -> 26.4 us
    ppermute x1, waiting for transfers between devices: 2.58 us -> 9.06 us  [body(): from_right = lax.ppermute(tokens, 'tp', ring(4, 3))]
    ppermute x2, waiting for transfers between devices: 4.11 us -> 0.01 us  [the longest x1 0.01 us: body(): far_b = lax.ppermute(from_left[2 * n // 3:], 'tp', ring(4, 3))]
    ppermute x3, waiting for transfers between devices: 6.65 us -> 3.75 us  [body(): plane.append(lax.ppermute(load, 'sp', grid_move(k, False)))]
    ppermute x3, starting transfers between devices: 2.59 us -> 5.49 us  [body(): rows_in.append(lax.ppermute(mine, 'tp', ring(4, k)))]
    unnamed x18 -> x16, local copies, waits for them, and re-layouts: 5.37 us -> 5.36 us
  transfers between devices with their start and end apart: 23 -> 23, of which waited for: 11 -> 8; matrix products, arithmetic and copies ran while one was open for 0% -> 1% of each run, Pallas kernels for 74% -> 73%
where the time goes in v3:
time: 221 us; the launch traced here: 220 us
  Pallas kernels  162 us (73%)
  starting transfers between devices  26.4 us (12%)
  waiting for transfers between devices  24.3 us (11%)
  local copies, waits for them, and re-layouts  5.39 us (2%)
    pallas_call x4, Pallas kernels, attend(): pl.pallas_call(functools.partial(attend_kernel, n_kv=len(kvs), n_extra=le...  156 us
    ppermute x1, waiting for transfers between devices, body(): from_right = lax.ppermute(tokens, 'tp', ring(4, 3))  9.06 us
    ppermute x3, starting transfers between devices, body(): rows_in.append(lax.ppermute(mine, 'tp', ring(4, k)))  5.49 us
    unnamed x16, local copies, waits for them, and re-layouts  5.36 us
    ppermute x3, starting transfers between devices, body(): line.append(lax.ppermute(kv, 'sp', grid_move(k, True)))  4.97 us
    ppermute x3, waiting for transfers between devices, body(): line.append(lax.ppermute(kv, 'sp', grid_move(k, True)))  4.8 us
    ppermute x3, waiting for transfers between devices, body(): rows_in.append(lax.ppermute(mine, 'tp', ring(4, k)))  4.72 us
  transfers between devices with their start and end apart: 23, of which 8 were waited for; matrix products, arithmetic and copies ran while one was open for 1% of the time, Pallas kernels for 73%

profile of v3, /device:TPU:0, one launch (start us, length us, event | category | flops | bytes accessed | tf_op | source)
XLA Modules:
  0.0 220.4 jit_solution(9293220238929392916)
XLA Ops:
  0.6 2.9 %collective-permute-start = (bf16[96,2048]{1,0:T(8,128)(2,1)}, bf16[96,2048]{1,0:T(8,128)(2,1)S(1)}, u32[]{:S(2)}, u32[]{:S(2)}) collective-permute-start(bf16[96,2048]{1,0:T(8,128)(2,1)} %t0.1), channel_id=1, source_target_pairs={{0,3},{1,2},{2,1},{3,0},{4,7},{5,6},{6,5},{7,4},{8,11},{9,10},{10,... | collective-permute-start | bytes 1179656 | tf_op jit(solution)/shard_map/ppermute | solution.py:307
  3.6 0.2 collective-permute-start.2
  3.8 0.0 copy-start.7
  3.8 9.1 %collective-permute-done.t2 = bf16[96,2048]{1,0:T(8,128)(2,1)S(1)} collective-permute-done((bf16[96,2048]{1,0:T(8,128)(2,1)}, bf16[96,2048]{1,0:T(8,128)(2,1)S(1)}, u32[]{:S(2)}, u32[]{:S(2)}) %collective-permute-start) | collective-permute-done | bytes 393248 | tf_op jit(solution)/shard_map/ppermute | solution.py:307
  12.9 0.6 collective-permute-start.1
  13.5 1.1 sine_select_fusion.tab
  14.6 0.0 collective-permute-done.2.t1
  14.6 2.6 %collective-permute-start.3 = (bf16[32,2048]{1,0:T(8,128)(2,1)S(1)}, bf16[32,2048]{1,0:T(8,128)(2,1)S(1)}, u32[]{:S(2)}, u32[]{:S(2)}) collective-permute-start(bf16[32,2048]{1,0:T(8,128)(2,1)S(1)} %slice.9), channel_id=1, source_target_pairs={{0,3},{1,2},{2,1},{3,0},{4,7},{5,6},{6,5},{7,4},{8,11},{9,10},{10,... | collective-permute-start | bytes 393224 | tf_op jit(solution)/shard_map/ppermute | solution.py:309
  17.2 0.1 pad_add_fusion.place
  17.3 1.2 copy-done
  18.5 1.2 copy-done.2
  19.7 1.0 copy-done.3
  20.7 0.9 copy-done.4
  21.7 0.9 copy-done.5
  22.6 1.1 shard_map.95
  23.7 0.0 copy-start.6
  23.7 0.7 shard_map.96.raw_near
  24.4 0.0 collective-permute-done.3.t4
  24.4 0.0 collective-permute-done.1.t3
  24.4 0.6 shard_map.97
  25.0 3.9 %collective-permute-start.6 = (bf16[384,128]{1,0:T(8,128)(2,1)S(1)}, bf16[384,128]{1,0:T(8,128)(2,1)S(1)}, u32[]{:S(2)}, u32[]{:S(2)}) collective-permute-start(bf16[384,128]{1,0:T(8,128)(2,1)S(1)} %get-tuple-element.31.refs_0_), channel_id=1, source_target_pairs={{0,64},{4,20},{8,72},{12,28},{16,80},{20,4},{24,88},{28,12},{32,96... | collective-permute-start | bytes 294920 | tf_op jit(solution)/shard_map/ppermute | solution.py:343
  29.0 0.7 collective-permute-start.5
  29.7 0.3 collective-permute-start.4
  30.0 1.6 collective-permute-done.6.refs_3_
  31.6 3.2 %collective-permute-done.5.refs_2_ = bf16[384,128]{1,0:T(8,128)(2,1)S(1)} collective-permute-done((bf16[384,128]{1,0:T(8,128)(2,1)S(1)}, bf16[384,128]{1,0:T(8,128)(2,1)S(1)}, u32[]{:S(2)}, u32[]{:S(2)}) %collective-permute-start.5) | collective-permute-done | bytes 98336 | tf_op jit(solution)/shard_map/ppermute | solution.py:343
  34.8 0.0 collective-permute-done.4.refs_1_
  34.8 0.1 collective-permute-start.13
  34.9 3.3 %collective-permute-start.11 = (bf16[1536,128]{1,0:T(8,128)(2,1)S(1)}, bf16[1536,128]{1,0:T(8,128)(2,1)S(1)}, u32[]{:S(2)}, u32[]{:S(2)}) collective-permute-start(bf16[1536,128]{1,0:T(8,128)(2,1)S(1)} %shard_map.99.refs_1_.refs_4_), channel_id=1, source_target_pairs={{0,16},{4,68},{8,24},{12,76},{16,0},{20,84},{24,8},{28,92},{32,48}... | collective-permute-start | bytes 1179656 | tf_op jit(solution)/shard_map/ppermute | solution.py:356
  38.2 1.1 collective-permute-start.9
  39.3 0.0 collective-permute-start.7
  39.3 1.5 collective-permute-start.16
  40.7 0.0 collective-permute-done.13.refs_2_.refs_5_
  40.7 2.6 %collective-permute-start.15 = (bf16[128,2048]{1,0:T(8,128)(2,1)S(1)}, bf16[128,2048]{1,0:T(8,128)(2,1)S(1)}, u32[]{:S(2)}, u32[]{:S(2)}) collective-permute-start(bf16[128,2048]{1,0:T(8,128)(2,1)S(1)} %get-tuple-element.44), channel_id=1, source_target_pairs={{0,3},{1,2},{2,1},{3,0},{4,7},{5,6},{6,5},{7,4},{8,11},{9,10},{10,... | collective-permute-start | bytes 1572872 | tf_op jit(solution)/shard_map/ppermute | solution.py:365
  43.3 1.0 collective-permute-done.11.refs_3_.refs_8_
  44.4 1.4 collective-permute-start.14
  45.8 2.7 %collective-permute-done.9.refs_2_.refs_7_ = bf16[1536,128]{1,0:T(8,128)(2,1)S(1)} collective-permute-done((bf16[1536,128]{1,0:T(8,128)(2,1)S(1)}, bf16[1536,128]{1,0:T(8,128)(2,1)S(1)}, u32[]{:S(2)}, u32[]{:S(2)}) %collective-permute-start.9) | collective-permute-done | bytes 393248 | tf_op jit(solution)/shard_map/ppermute | solution.py:356
  48.5 0.0 collective-permute-start.12
  48.5 0.4 shard_map.98.refs_0_
  48.9 4.7 %shard_map.100 = (f32[64,1536]{1,0:T(8,128)S(1)}, f32[8,1536]{1,0:T(8,128)S(1)}, f32[1,1536]{1,0:T(1,128)S(1)}) custom-call(bf16[128,1536]{1,0:T(8,128)(2,1)S(1)} %shard_map.98.refs_0_, bf16[1536,128]{1,0:T(8,128)(2,1)S(1)} %shard_map.99.refs_1_.refs_4_, bf16[1536,128]{1,0:T(8,128)(2,1)S(1)} %collective-permute-done.13.refs_2_.refs_5_), custom_call_target="tpu_custom_call" | custom-call | flops 1207959552 | bytes 1572864 | tf_op jit(solution)/shard_map/pallas_call | solution.py:258
  53.5 0.0 collective-permute-done.7.refs_1_.refs_6_
  53.5 6.4 %shard_map.101 = (f32[64,1536]{1,0:T(8,128)S(1)}, f32[8,1536]{1,0:T(8,128)S(1)}, f32[1,1536]{1,0:T(1,128)S(1)}) custom-call(bf16[128,1536]{1,0:T(8,128)(2,1)S(1)} %shard_map.98.refs_0_, bf16[1536,128]{1,0:T(8,128)(2,1)S(1)} %collective-permute-done.7.refs_1_.refs_6_, bf16[1536,128]{1,0:T(8,128)(2,1)S(1)} %collective-permute-done.9.refs_2_.refs_7_, ...), custom_call_target="tpu_custom_call" | custom-call | flops 1811939328 | bytes 1966080 | tf_op jit(solution)/shard_map/pallas_call | solution.py:258
  59.9 0.0 collective-permute-done.16.w3
  59.9 4.7 %collective-permute-done.15.w2 = bf16[128,2048]{1,0:T(8,128)(2,1)S(1)} collective-permute-done((bf16[128,2048]{1,0:T(8,128)(2,1)S(1)}, bf16[128,2048]{1,0:T(8,128)(2,1)S(1)}, u32[]{:S(2)}, u32[]{:S(2)}) %collective-permute-start.15) | collective-permute-done | bytes 524320 | tf_op jit(solution)/shard_map/ppermute | solution.py:365
  64.6 0.0 collective-permute-done.14.w1
  64.6 0.0 collective-permute-start.17
  64.7 0.5 collective-permute-start.10
  65.2 0.0 collective-permute-start.8
  65.2 0.5 collective-permute-start.18
  65.7 0.0 collective-permute-done.12.refs_3_
  65.7 0.0 collective-permute-start.19
  65.7 1.4 collective-permute-done.10.refs_2_
  67.1 0.6 collective-permute-done.8.refs_1_
  67.7 81.9 %shard_map.102 = (bf16[96,256]{1,0:T(8,128)(2,1)S(1)}, bf16[96,256]{1,0:T(8,128)(2,1)S(1)}, bf16[96,256]{1,0:T(8,128)(2,1)S(1)}, f32[4,96]{1,0:T(4,128)S(1)}, f32[4,96]{1,0:T(4,128)S(1)}, /*index=5*/f32[4,96]{1,0:T(4,128)S(1)}) custom-call(bf16[128,1536]{1,0:T(8,128)(2,1)S(1)} %shard_map.98.refs_0_, bf16[1536,128]{1,0:T(8,128)(2,1)S(1)} %collective-permute-done.8.refs_1_, ...), custom_call_target="tpu_custom_call" | custom-call | flops 1358954496 | bytes 1769472 | tf_op jit(solution)/shard_map/pallas_call | solution.py:258
  149.6 0.0 copy-start.1
  149.6 0.1 collective-permute-start.20
  149.7 2.6 %collective-permute-start.21 = (bf16[96,256]{1,0:T(8,128)(2,1)S(1)}, bf16[96,256]{1,0:T(8,128)(2,1)S(1)}, u32[]{:S(2)}, u32[]{:S(2)}) collective-permute-start(bf16[96,256]{1,0:T(8,128)(2,1)S(1)} %get-tuple-element.50), channel_id=1, source_target_pairs={{0,3},{1,2},{2,1},{3,0},{4,7},{5,6},{6,5},{7,4},{8,11},{9,10},{10,... | collective-permute-start | bytes 147464 | tf_op jit(solution)/shard_map/ppermute | solution.py:383
  152.3 1.5 collective-permute-start.22
  153.8 63.5 %shard_map.103 = (bf16[96,256]{1,0:T(8,128)(2,1)S(1)}, f32[4,96]{1,0:T(4,128)S(1)}) custom-call(bf16[128,1536]{1,0:T(8,128)(2,1)S(1)} %shard_map.98.refs_0_, bf16[1536,128]{1,0:T(8,128)(2,1)S(1)} %collective-permute-done.8.refs_1_, bf16[1536,128]{1,0:T(8,128)(2,1)S(1)} %collective-permute-done.10.refs_2_, ...), custom_call_target="tpu_custom_call" | custom-call | flops 452984832 | bytes 1376256 | tf_op jit(solution)/shard_map/pallas_call | solution.py:258
  217.3 0.0 collective-permute-done.19.x3
  217.3 1.6 shard_map.104
  218.9 0.0 collective-permute-done.20.a1
  218.9 0.0 collective-permute-done.21.a2
  219.0 0.0 collective-permute-done.22.a3
  219.0 1.4 shard_map.105
  (16 shorter events, 0.1 us)
Async XLA Ops:
  0.6 12.3 %collective-permute-start = (bf16[96,2048]{1,0:T(8,128)(2,1)}, bf16[96,2048]{1,0:T(8,128)(2,1)S(1)}, u32[]{:S(2)}, u32[]{:S(2)}) collective-permute-start(bf16[96,2048]{1,0:T(8,128)(2,1)} %t0.1), channel_id=1, source_target_pairs={{0,3},{1,2},{2,1},{3,0},{4,7},{5,6},{6,5},{7,4},{8,11},{9,10},{10,... | collective-permute-start | bytes 1179656 | tf_op jit(solution)/shard_map/ppermute | solution.py:307
  3.6 11.0 %collective-permute-start.2 = (bf16[96,2048]{1,0:T(8,128)(2,1)}, bf16[96,2048]{1,0:T(8,128)(2,1)S(1)}, u32[]{:S(2)}, u32[]{:S(2)}) collective-permute-start(bf16[96,2048]{1,0:T(8,128)(2,1)} %t0.1), channel_id=1, source_target_pairs={{0,1},{1,0},{2,3},{3,2},{4,5},{5,4},{6,7},{7,6},{8,9},{9,8},{10,11... | collective-permute-start | bytes 1179656 | tf_op jit(solution)/shard_map/ppermute | solution.py:306
  3.8 20.6 %copy-start.7 = (bf16[1,64]{1,0:T(2,128)(2,1)S(1)}, bf16[1,64]{1,0:T(2,128)(2,1)}, u32[]{:S(2)}) copy-start(bf16[1,64]{1,0:T(2,128)(2,1)} %gk.1) | copy-start | bytes 388
  12.9 11.5 %collective-permute-start.1 = (bf16[64,2048]{1,0:T(8,128)(2,1)S(1)}, bf16[64,2048]{1,0:T(8,128)(2,1)S(1)}, u32[]{:S(2)}, u32[]{:S(2)}) collective-permute-start(bf16[64,2048]{1,0:T(8,128)(2,1)S(1)} %slice.8), channel_id=1, source_target_pairs={{0,1},{1,0},{2,3},{3,2},{4,5},{5,4},{6,7},{7,6},{8,9},{9,8},{10,11... | collective-permute-start | bytes 786440 | tf_op jit(solution)/shard_map/ppermute | solution.py:308
  14.6 9.8 %collective-permute-start.3 = (bf16[32,2048]{1,0:T(8,128)(2,1)S(1)}, bf16[32,2048]{1,0:T(8,128)(2,1)S(1)}, u32[]{:S(2)}, u32[]{:S(2)}) collective-permute-start(bf16[32,2048]{1,0:T(8,128)(2,1)S(1)} %slice.9), channel_id=1, source_target_pairs={{0,3},{1,2},{2,1},{3,0},{4,7},{5,6},{6,5},{7,4},{8,11},{9,10},{10,... | collective-permute-start | bytes 393224 | tf_op jit(solution)/shard_map/ppermute | solution.py:309
  17.3 1.2 copy-start
  18.5 1.2 copy-start.2
  19.7 1.0 copy-start.3
  20.7 0.9 copy-start.4
  21.7 0.9 copy-start.5
  23.7 24.8 %copy-start.6 = (bf16[4,64]{1,0:T(4,128)(2,1)S(1)}, bf16[4,64]{1,0:T(4,128)(2,1)}, u32[]{:S(2)}) copy-start(bf16[4,64]{1,0:T(4,128)(2,1)} %gq.1) | copy-start | bytes 1540
  25.0 6.5 %collective-permute-start.6 = (bf16[384,128]{1,0:T(8,128)(2,1)S(1)}, bf16[384,128]{1,0:T(8,128)(2,1)S(1)}, u32[]{:S(2)}, u32[]{:S(2)}) collective-permute-start(bf16[384,128]{1,0:T(8,128)(2,1)S(1)} %get-tuple-element.31.refs_0_), channel_id=1, source_target_pairs={{0,64},{4,20},{8,72},{12,28},{16,80},{20,4},{24,88},{28,12},{32,96... | collective-permute-start | bytes 294920 | tf_op jit(solution)/shard_map/ppermute | solution.py:343
  29.0 5.8 %collective-permute-start.5 = (bf16[384,128]{1,0:T(8,128)(2,1)S(1)}, bf16[384,128]{1,0:T(8,128)(2,1)S(1)}, u32[]{:S(2)}, u32[]{:S(2)}) collective-permute-start(bf16[384,128]{1,0:T(8,128)(2,1)S(1)} %get-tuple-element.31.refs_0_), channel_id=1, source_target_pairs={{0,96},{4,28},{8,104},{12,20},{16,112},{20,12},{24,120},{28,4},{32... | collective-permute-start | bytes 294920 | tf_op jit(solution)/shard_map/ppermute | solution.py:343
  29.7 5.1 %collective-permute-start.4 = (bf16[384,128]{1,0:T(8,128)(2,1)S(1)}, bf16[384,128]{1,0:T(8,128)(2,1)S(1)}, u32[]{:S(2)}, u32[]{:S(2)}) collective-permute-start(bf16[384,128]{1,0:T(8,128)(2,1)S(1)} %get-tuple-element.31.refs_0_), channel_id=1, source_target_pairs={{0,32},{4,12},{8,40},{12,4},{16,48},{20,28},{24,56},{28,20},{32,0}... | collective-permute-start | bytes 294920 | tf_op jit(solution)/shard_map/ppermute | solution.py:343
  34.8 5.9 %collective-permute-start.13 = (bf16[1536,128]{1,0:T(8,128)(2,1)S(1)}, bf16[1536,128]{1,0:T(8,128)(2,1)S(1)}, u32[]{:S(2)}, u32[]{:S(2)}) collective-permute-start(bf16[1536,128]{1,0:T(8,128)(2,1)S(1)} %shard_map.99.refs_1_.refs_4_), channel_id=1, source_target_pairs={{0,4},{4,0},{8,12},{12,8},{16,20},{20,16},{24,28},{28,24},{32,36},... | collective-permute-start | bytes 1179656 | tf_op jit(solution)/shard_map/ppermute | solution.py:357
  34.9 9.5 %collective-permute-start.11 = (bf16[1536,128]{1,0:T(8,128)(2,1)S(1)}, bf16[1536,128]{1,0:T(8,128)(2,1)S(1)}, u32[]{:S(2)}, u32[]{:S(2)}) collective-permute-start(bf16[1536,128]{1,0:T(8,128)(2,1)S(1)} %shard_map.99.refs_1_.refs_4_), channel_id=1, source_target_pairs={{0,16},{4,68},{8,24},{12,76},{16,0},{20,84},{24,8},{28,92},{32,48}... | collective-permute-start | bytes 1179656 | tf_op jit(solution)/shard_map/ppermute | solution.py:356
  38.2 10.3 %collective-permute-start.9 = (bf16[1536,128]{1,0:T(8,128)(2,1)S(1)}, bf16[1536,128]{1,0:T(8,128)(2,1)S(1)}, u32[]{:S(2)}, u32[]{:S(2)}) collective-permute-start(bf16[1536,128]{1,0:T(8,128)(2,1)S(1)} %shard_map.99.refs_1_.refs_4_), channel_id=1, source_target_pairs={{0,24},{4,100},{8,16},{12,108},{16,8},{20,116},{24,0},{28,124},{32... | collective-permute-start | bytes 1179656 | tf_op jit(solution)/shard_map/ppermute | solution.py:356
  39.3 14.3 %collective-permute-start.7 = (bf16[1536,128]{1,0:T(8,128)(2,1)S(1)}, bf16[1536,128]{1,0:T(8,128)(2,1)S(1)}, u32[]{:S(2)}, u32[]{:S(2)}) collective-permute-start(bf16[1536,128]{1,0:T(8,128)(2,1)S(1)} %shard_map.99.refs_1_.refs_4_), channel_id=1, source_target_pairs={{0,8},{4,36},{8,0},{12,44},{16,24},{20,52},{24,16},{28,60},{32,40}... | collective-permute-start | bytes 1179656 | tf_op jit(solution)/shard_map/ppermute | solution.py:356
  39.3 20.7 %collective-permute-start.16 = (bf16[128,2048]{1,0:T(8,128)(2,1)S(1)}, bf16[128,2048]{1,0:T(8,128)(2,1)S(1)}, u32[]{:S(2)}, u32[]{:S(2)}) collective-permute-start(bf16[128,2048]{1,0:T(8,128)(2,1)S(1)} %get-tuple-element.44), channel_id=1, source_target_pairs={{0,2},{1,3},{2,0},{3,1},{4,6},{5,7},{6,4},{7,5},{8,10},{9,11},{10,... | collective-permute-start | bytes 1572872 | tf_op jit(solution)/shard_map/ppermute | solution.py:365
  40.7 23.9 %collective-permute-start.15 = (bf16[128,2048]{1,0:T(8,128)(2,1)S(1)}, bf16[128,2048]{1,0:T(8,128)(2,1)S(1)}, u32[]{:S(2)}, u32[]{:S(2)}) collective-permute-start(bf16[128,2048]{1,0:T(8,128)(2,1)S(1)} %get-tuple-element.44), channel_id=1, source_target_pairs={{0,3},{1,2},{2,1},{3,0},{4,7},{5,6},{6,5},{7,4},{8,11},{9,10},{10,... | collective-permute-start | bytes 1572872 | tf_op jit(solution)/shard_map/ppermute | solution.py:365
  44.4 20.3 %collective-permute-start.14 = (bf16[128,2048]{1,0:T(8,128)(2,1)S(1)}, bf16[128,2048]{1,0:T(8,128)(2,1)S(1)}, u32[]{:S(2)}, u32[]{:S(2)}) collective-permute-start(bf16[128,2048]{1,0:T(8,128)(2,1)S(1)} %get-tuple-element.44), channel_id=1, source_target_pairs={{0,1},{1,0},{2,3},{3,2},{4,5},{5,4},{6,7},{7,6},{8,9},{9,8},{10,11... | collective-permute-start | bytes 1572872 | tf_op jit(solution)/shard_map/ppermute | solution.py:365
  48.5 17.2 %collective-permute-start.12 = (bf16[1536,128]{1,0:T(8,128)(2,1)S(1)}, bf16[1536,128]{1,0:T(8,128)(2,1)S(1)}, u32[]{:S(2)}, u32[]{:S(2)}) collective-permute-start(bf16[1536,128]{1,0:T(8,128)(2,1)S(1)} %collective-permute-done.11.refs_3_.refs_8_), channel_id=1, source_target_pairs={{0,4},{4,0},{8,12},{12,8},{16,20},{20,16},{24,28},{28,24},{32,36},... | collective-permute-start | bytes 1179656 | tf_op jit(solution)/shard_map/ppermute | solution.py:360
  64.6 87.7 %collective-permute-start.17 = (bf16[128,2048]{1,0:T(8,128)(2,1)S(1)}, bf16[128,2048]{1,0:T(8,128)(2,1)S(1)}, u32[]{:S(2)}, u32[]{:S(2)}) collective-permute-start(bf16[128,2048]{1,0:T(8,128)(2,1)S(1)} %collective-permute-done.14.w1), channel_id=1, source_target_pairs={{0,4},{4,0},{8,12},{12,8},{16,20},{20,16},{24,28},{28,24},{32,36},... | collective-permute-start | bytes 1572872 | tf_op jit(solution)/shard_map/ppermute | solution.py:375
  64.7 2.5 %collective-permute-start.10 = (bf16[1536,128]{1,0:T(8,128)(2,1)S(1)}, bf16[1536,128]{1,0:T(8,128)(2,1)S(1)}, u32[]{:S(2)}, u32[]{:S(2)}) collective-permute-start(bf16[1536,128]{1,0:T(8,128)(2,1)S(1)} %collective-permute-done.9.refs_2_.refs_7_), channel_id=1, source_target_pairs={{0,4},{4,0},{8,12},{12,8},{16,20},{20,16},{24,28},{28,24},{32,36},... | collective-permute-start | bytes 1179656 | tf_op jit(solution)/shard_map/ppermute | solution.py:360
  65.2 2.5 %collective-permute-start.8 = (bf16[1536,128]{1,0:T(8,128)(2,1)S(1)}, bf16[1536,128]{1,0:T(8,128)(2,1)S(1)}, u32[]{:S(2)}, u32[]{:S(2)}) collective-permute-start(bf16[1536,128]{1,0:T(8,128)(2,1)S(1)} %collective-permute-done.7.refs_1_.refs_6_), channel_id=1, source_target_pairs={{0,4},{4,0},{8,12},{12,8},{16,20},{20,16},{24,28},{28,24},{32,36},... | collective-permute-start | bytes 1179656 | tf_op jit(solution)/shard_map/ppermute | solution.py:360
  65.2 152.1 %collective-permute-start.18 = (bf16[128,2048]{1,0:T(8,128)(2,1)S(1)}, bf16[128,2048]{1,0:T(8,128)(2,1)S(1)}, u32[]{:S(2)}, u32[]{:S(2)}) collective-permute-start(bf16[128,2048]{1,0:T(8,128)(2,1)S(1)} %collective-permute-done.15.w2), channel_id=1, source_target_pairs={{0,4},{4,0},{8,12},{12,8},{16,20},{20,16},{24,28},{28,24},{32,36},... | collective-permute-start | bytes 1572872 | tf_op jit(solution)/shard_map/ppermute | solution.py:375
  65.7 151.6 %collective-permute-start.19 = (bf16[128,2048]{1,0:T(8,128)(2,1)S(1)}, bf16[128,2048]{1,0:T(8,128)(2,1)S(1)}, u32[]{:S(2)}, u32[]{:S(2)}) collective-permute-start(bf16[128,2048]{1,0:T(8,128)(2,1)S(1)} %collective-permute-done.16.w3), channel_id=1, source_target_pairs={{0,4},{4,0},{8,12},{12,8},{16,20},{20,16},{24,28},{28,24},{32,36},... | collective-permute-start | bytes 1572872 | tf_op jit(solution)/shard_map/ppermute | solution.py:375
  149.6 67.7 %copy-start.1 = (bf16[256,2048]{1,0:T(8,128)(2,1)S(1)}, bf16[256,2048]{1,0:T(8,128)(2,1)}, u32[]{:S(2)}) copy-start(bf16[256,2048]{1,0:T(8,128)(2,1)} %w0.1) | copy-start | bytes 3145732
  149.6 69.3 %collective-permute-start.20 = (bf16[96,256]{1,0:T(8,128)(2,1)S(1)}, bf16[96,256]{1,0:T(8,128)(2,1)S(1)}, u32[]{:S(2)}, u32[]{:S(2)}) collective-permute-start(bf16[96,256]{1,0:T(8,128)(2,1)S(1)} %get-tuple-element.49), channel_id=1, source_target_pairs={{0,1},{1,0},{2,3},{3,2},{4,5},{5,4},{6,7},{7,6},{8,9},{9,8},{10,11... | collective-permute-start | bytes 147464 | tf_op jit(solution)/shard_map/ppermute | solution.py:383
  149.7 69.2 %collective-permute-start.21 = (bf16[96,256]{1,0:T(8,128)(2,1)S(1)}, bf16[96,256]{1,0:T(8,128)(2,1)S(1)}, u32[]{:S(2)}, u32[]{:S(2)}) collective-permute-start(bf16[96,256]{1,0:T(8,128)(2,1)S(1)} %get-tuple-element.50), channel_id=1, source_target_pairs={{0,3},{1,2},{2,1},{3,0},{4,7},{5,6},{6,5},{7,4},{8,11},{9,10},{10,... | collective-permute-start | bytes 147464 | tf_op jit(solution)/shard_map/ppermute | solution.py:383
  152.3 66.6 %collective-permute-start.22 = (bf16[96,256]{1,0:T(8,128)(2,1)S(1)}, bf16[96,256]{1,0:T(8,128)(2,1)S(1)}, u32[]{:S(2)}, u32[]{:S(2)}) collective-permute-start(bf16[96,256]{1,0:T(8,128)(2,1)S(1)} %get-tuple-element.51), channel_id=1, source_target_pairs={{0,2},{1,3},{2,0},{3,1},{4,6},{5,7},{6,4},{7,5},{8,10},{9,11},{10,... | collective-permute-start | bytes 147464 | tf_op jit(solution)/shard_map/ppermute | solution.py:383
